TPU v7x, 32 devices: a whole 2x2x4 slice. The times are simulated.
32 devices in a mesh: ep: 8 (over z, core), tp: 4 (over y, x).
Axes of the slice: x: 2, y: 2, z: 4, core: 2. Of those that a mesh axis runs over, the one named last changes fastest.
Arguments:
- tokens: bfloat16 [1024, 2048], P('ep'), may hold values from -6 to 6
- cotangent: bfloat16 [1024, 2048], P('ep'), may hold values from -6 to 6
- routes: int32 [1024, 2], P('ep'), may hold values from 0 to 7, all different within a row; in each aligned block of 128 rows (0 to 127, 128 to 255, ...) at most 64 rows name the same one
- route_weight: float32 [1024, 2], P('ep'), may hold values from 0.1 to 1
- w_gate: bfloat16 [8, 2048, 1024], P('ep', None, 'tp'), may hold values from -0.1875 to 0.1875
- w_up: bfloat16 [8, 2048, 1024], P('ep', None, 'tp'), may hold values from -0.1875 to 0.1875
- w_down: bfloat16 [8, 1024, 2048], P('ep', 'tp'), may hold values from -0.1875 to 0.1875
Outputs:
- grad_tokens: bfloat16 [1024, 2048], P('ep', 'tp')
- grad_route_weight: float32 [1024, 2], P('ep')
- grad_gate: float32 [8, 2048, 1024], P('ep', None, 'tp')
- grad_up: float32 [8, 2048, 1024], P('ep', None, 'tp')
- grad_down: float32 [8, 1024, 2048], P('ep', 'tp')
Inputs may be any that keep to these rules, and one draw needn't show every extreme that they name: `routes`: each row names 2 different experts. In each aligned block of 128 rows (the rows of one index of ep) no expert is named by more than 64 rows, and in every draw some expert is named by exactly 64 rows of some block.
All inputs are finite; a program needn't handle non-finite values.
Results may differ from a plain program's by a relative error of at most 0.023.
Values may be sent and summed in bfloat16 or wider, within the bound.
A program may use at most 64 MiB of HBM per device.

v0:
```python
import functools

import jax
import jax.numpy as jnp
from jax import lax
from jax.experimental import pallas as pl
from jax.experimental.pallas import tpu as pltpu
from jax.sharding import PartitionSpec as P


def slot_index(block_routes, experts, capacity):
    flat_ids = block_routes.reshape(-1)
    onehot = (flat_ids[:, None] == jnp.arange(experts, dtype=jnp.int32)[None, :]).astype(jnp.int32)
    earlier = jnp.cumsum(onehot, axis=0) - onehot
    return flat_ids * capacity + jnp.sum(earlier * onehot, axis=1)


def slotted(tokens, cotangent, routes, route_weight, w_gate, w_up, w_down):
    f32 = jnp.float32
    tok_rows, model_width = tokens.shape
    choices_row = routes.shape[1]
    experts = lax.axis_size("ep")
    capacity = 2 * tok_rows * choices_row // experts
    recv_rows = experts * capacity
    slot_ids = slot_index(routes, experts, capacity)
    send_w = jnp.zeros((recv_rows,), f32).at[slot_ids].set(route_weight.reshape(-1))
    send_x = (
        jnp.zeros((recv_rows, model_width), jnp.bfloat16)
        .at[slot_ids]
        .set(jnp.repeat(tokens, choices_row, axis=0))
    )
    send_dy = (
        jnp.zeros((recv_rows, model_width), jnp.bfloat16)
        .at[slot_ids]
        .set(jnp.repeat(cotangent, choices_row, axis=0))
    )
    got_x = lax.all_to_all(
        send_x.reshape(experts, capacity, model_width),
        "ep",
        split_axis=0,
        concat_axis=0,
        tiled=True,
    )
    got_dy, got_w = (
        lax.all_to_all(
            send_dy.reshape(experts, capacity, model_width),
            "ep",
            split_axis=0,
            concat_axis=0,
            tiled=True,
        ),
        lax.all_to_all(
            send_w.reshape(experts, capacity, 1).astype(jnp.bfloat16),
            "ep",
            split_axis=0,
            concat_axis=0,
            tiled=True,
        ).astype(jnp.float32),
    )
    rows_x = got_x.reshape(recv_rows, model_width)
    rows_dy = got_dy.reshape(recv_rows, model_width)
    rows_w = got_w.reshape(recv_rows)
    gate_w = w_gate[0]
    up_w = w_up[0]
    down_w = w_down[0]
    gate_pre = jnp.dot(rows_x, gate_w, preferred_element_type=f32)
    up_pre = jnp.dot(rows_x, up_w, preferred_element_type=f32)
    gate_sig = jax.nn.sigmoid(gate_pre)
    act_full = gate_pre * gate_sig * up_pre
    act = act_full.astype(jnp.bfloat16)
    back_hidden = jnp.einsum("rd,fd->rf", rows_dy, down_w, preferred_element_type=f32)
    weighted_cot = (rows_w[:, None] * rows_dy.astype(f32)).astype(jnp.bfloat16)
    d_hidden = rows_w[:, None] * back_hidden
    d_gate = (d_hidden * up_pre * gate_sig * (1.0 + gate_pre * (1.0 - gate_sig))).astype(
        jnp.bfloat16
    )
    d_up = (d_hidden * gate_pre * gate_sig).astype(jnp.bfloat16)
    gate_part = jnp.sum(act_full * back_hidden, axis=1)
    token_part = jnp.einsum("rf,df->rd", d_gate, gate_w, preferred_element_type=f32)
    token_part = token_part + jnp.einsum("rf,df->rd", d_up, up_w, preferred_element_type=f32)
    grad_gate = jnp.einsum("rd,rf->df", rows_x, d_gate, preferred_element_type=f32)[None]
    grad_up = jnp.einsum("rd,rf->df", rows_x, d_up, preferred_element_type=f32)[None]
    grad_down = jnp.einsum("rf,rd->fd", act, weighted_cot, preferred_element_type=f32)[None]
    rounded_part = token_part.astype(jnp.bfloat16).astype(f32)
    shares = lax.psum_scatter(
        rounded_part.astype(jnp.bfloat16), "tp", scatter_dimension=1, tiled=True
    )
    gate_total = lax.psum(gate_part, "tp")
    back_x, back_gate = (
        lax.all_to_all(
            shares.reshape(experts, capacity, -1), "ep", split_axis=0, concat_axis=0, tiled=True
        ),
        lax.all_to_all(
            gate_total.reshape(experts, capacity).astype(jnp.bfloat16),
            "ep",
            split_axis=0,
            concat_axis=0,
            tiled=True,
        ).astype(jnp.float32),
    )
    picked = back_x.reshape(recv_rows, -1)[slot_ids].astype(f32).reshape(tok_rows, choices_row, -1)
    grad_route_weight = back_gate.reshape(recv_rows)[slot_ids].reshape(tok_rows, choices_row)
    grad_tokens = jnp.sum(picked, axis=1).astype(jnp.bfloat16)
    return (grad_tokens, grad_route_weight, grad_gate, grad_up, grad_down)


def kernel(ep, tp, tokens, cotangent, table, w_gate, w_up, w_down,
           out_tok, out_home, out_gate, out_up, out_down,
           full, gate_v, up_v, down_v, weights, part, other, top, bottom,
           in_top, in_bottom, last_top, last_bottom, share, arrived,
           d_gate, d_up, act_w, g_gate, g_up, g_down, score, scores, total, home, result,
           local, sent, got):
    f32, bf16 = jnp.float32, jnp.bfloat16
    rows, width = tokens.shape
    cols = width // tp
    half = rows // 2
    nz = ep // 2
    e, t = lax.axis_index("ep"), lax.axis_index("tp")
    z, c = e // 2, lax.rem(e, 2)
    y, x = t // 2, lax.rem(t, 2)
    side = z * 2 + 1 - c
    tx, ty = y * 2 + 1 - x, (1 - y) * 2 + x
    td = (1 - y) * 2 + 1 - x
    slots, started, locals_ = {}, [], []

    def slot(*name):
        return got.at[slots.setdefault(name, len(slots))]

    def push(src, dst, name, to_e, to_t):
        copy = pltpu.make_async_remote_copy(
            src_ref=src, dst_ref=dst, send_sem=sent.at[len(started)], recv_sem=slot(*name),
            device_id={"ep": to_e, "tp": to_t}, device_id_type=pl.DeviceIdType.MESH)
        copy.start()
        started.append(copy)

    def landed(dst, *name):
        pltpu.make_async_remote_copy(
            src_ref=dst, dst_ref=dst, send_sem=sent.at[0], recv_sem=slot(*name),
            device_id={"ep": side, "tp": t}, device_id_type=pl.DeviceIdType.MESH).wait_recv()

    def bring(src, dst):
        copy = pltpu.make_async_copy(src, dst, local.at[len(locals_)])
        copy.start()
        locals_.append(copy)
        return copy

    own = [bring(ref.at[:, pl.ds(q * cols, cols)], full.at[e, a, q])
           for a, ref in enumerate((tokens, cotangent)) for q in range(tp)]
    loads = [bring(w_gate.at[0], gate_v), bring(w_up.at[0], up_v), bring(w_down.at[0], down_v)]
    weights[e] = table[...]

    barrier = pltpu.get_barrier_semaphore()
    for k in range(1, ep):
        pl.semaphore_signal(barrier, inc=1, device_id={"ep": lax.rem(e + k, ep), "tp": t},
                            device_id_type=pl.DeviceIdType.MESH)
    for k in range(1, tp):
        pl.semaphore_signal(barrier, inc=1, device_id={"ep": e, "tp": lax.rem(t + k, tp)},
                            device_id_type=pl.DeviceIdType.MESH)
    pl.semaphore_wait(barrier, ep + tp - 2)

    edge = jnp.minimum(z, nz - 1 - z)

    def back(i):
        near = z + (i + 1) // 2 * (1 - i % 2 * 2)
        away = jnp.where(z < nz - 1 - z, z + i - edge, z - i + edge)
        return jnp.where(i <= 2 * edge, near, away) if i else z

    relays = []

    def along(piece, from_z, a, go, to_z):
        copy = pltpu.make_async_remote_copy(
            src_ref=piece, dst_ref=piece, send_sem=sent.at[20 * nz + len(relays)],
            recv_sem=got.at[20 * nz + from_z * 2 + a],
            device_id={"ep": to_z * 2 + c, "tp": t}, device_id_type=pl.DeviceIdType.MESH)
        pl.when(go)(copy.start)
        relays.append((go, copy))

    for copy in own:
        copy.wait()
    for a in range(2):
        along(full.at[e, a, t], z, a, z < nz - 1, jnp.minimum(z + 1, nz - 1))
        along(full.at[e, a, t], z, a, z > 0, jnp.maximum(z - 1, 0))
    for a in range(2):
        push(full.at[e, a], full.at[e, a], ("side", 0, a), side, t)
    for k in range(1, ep):
        push(table, weights.at[e], ("w", k), lax.rem(e + k, ep), t)

    def spread(dz):
        s = back(dz) * 2 + c
        for a in range(2):
            piece = full.at[s, a, t]
            pltpu.make_async_remote_copy(
                src_ref=piece, dst_ref=piece, send_sem=sent.at[0],
                recv_sem=got.at[20 * nz + back(dz) * 2 + a],
                device_id={"ep": side, "tp": t}, device_id_type=pl.DeviceIdType.MESH).wait_recv()
            below = back(dz) < z
            go = jnp.where(below, z < nz - 1, z > 0)
            onward = jnp.where(below, jnp.minimum(z + 1, nz - 1), jnp.maximum(z - 1, 0))
            along(piece, back(dz), a, go, onward)
            push(piece, piece, ("x", dz, a), e, tx)
            push(piece, piece, ("y", dz, a), e, ty)

    def relay(dz):
        s = back(dz) * 2 + c
        piece = full.at[s, 0, ty]
        landed(piece, "y", dz, 0)
        push(piece, piece, ("d", dz, 0), e, tx)
        piece = full.at[s, 1, tx]
        landed(piece, "x", dz, 1)
        push(piece, piece, ("d", dz, 1), e, ty)

    def hand(dz):
        s = back(dz) * 2 + c
        landed(full.at[s, 0, tx], "x", dz, 0)
        landed(full.at[s, 0, td], "d", dz, 0)
        push(full.at[s, 0], full.at[s, 0], ("side", dz, 0), side, t)
        landed(full.at[s, 1, ty], "y", dz, 1)
        landed(full.at[s, 1, td], "d", dz, 1)
        push(full.at[s, 1], full.at[s, 1], ("side", dz, 1), side, t)

    def nt(a, b):
        return lax.dot_general(a, b, (((1,), (1,)), ((), ())), preferred_element_type=f32)

    def tn(a, b):
        return lax.dot_general(a, b, (((0,), (0,)), ((), ())), preferred_element_type=f32)

    def column(block):
        mine = lax.broadcasted_iota(jnp.int32, (ep, rows), 0) == e
        row = jnp.sum(jnp.where(mine, weights[block], 0.0), axis=0, keepdims=True)
        return jnp.transpose(jnp.broadcast_to(row, (rows, rows)))[:, :1]

    def compute(dz):
        b = back(dz) * 2
        for a in range(2):
            landed(full.at[back(dz) * 2 + 1 - c, a], "side", dz, a)
        g = u = bk = None
        for q in range(tp):
            span = pl.ds(q * cols, cols)
            xs = jnp.concatenate([full[b, 0, q], full[b + 1, 0, q]], axis=0)
            dy = jnp.concatenate([full[b, 1, q], full[b + 1, 1, q]], axis=0)
            g_q = jnp.dot(xs, gate_v[span, :], preferred_element_type=f32)
            u_q = jnp.dot(xs, up_v[span, :], preferred_element_type=f32)
            b_q = nt(dy, down_v[:, span])
            g, u, bk = (g_q, u_q, b_q) if q == 0 else (g + g_q, u + u_q, bk + b_q)
        w = jnp.concatenate([column(b), column(b + 1)], axis=0)
        sig = jax.nn.sigmoid(g)
        silu = g * sig
        act = silu * u
        d_h = w * bk
        dg = (d_h * u * sig * (1.0 + g * (1.0 - sig))).astype(bf16)
        du = (d_h * silu).astype(bf16)
        aw = (w * act).astype(bf16)
        sums = jnp.sum(act * bk, axis=1, keepdims=True)
        for i in range(2):
            cut = slice(i * rows, (i + 1) * rows)
            d_gate[b + i] = dg[cut]
            d_up[b + i] = du[cut]
            act_w[b + i] = aw[cut]
            score[b + i] = jnp.transpose(jnp.broadcast_to(sums[cut], (rows, rows)))[:8]
        for q in range(tp):
            span = pl.ds(q * cols, cols)
            piece = (nt(dg, gate_v[span, :]) + nt(du, up_v[span, :])).astype(bf16)
            part[b, q] = piece[:rows]
            part[b + 1, q] = piece[rows:]
        push(part.at[back(dz) * 2 + 1 - c], other.at[dz], ("pair", dz), side, t)

    for copy in loads:
        copy.wait()
    for k in range(1, ep):
        landed(weights.at[lax.rem(e - k + ep, ep)], "w", k)

    def add(*terms):
        value = terms[0].astype(f32)
        for term in terms[1:]:
            value = value + term.astype(f32)
        return value

    def first(dz):
        s = back(dz) * 2 + c
        landed(other.at[dz], "pair", dz)
        for r, q in enumerate((t, ty, tx, td)):
            top[dz, r] = add(part[s, q, :half], other[dz, q, :half]).astype(bf16)
        push(top.at[dz, pl.ds(2, 2)], in_top.at[dz], ("top", dz), e, tx)
        for r, q in enumerate((t, tx, ty, td)):
            bottom[dz, r] = add(part[s, q, half:], other[dz, q, half:]).astype(bf16)
        push(bottom.at[dz, pl.ds(2, 2)], in_bottom.at[dz], ("bottom", dz), e, ty)

    def second(dz):
        landed(in_top.at[dz], "top", dz)
        top[dz, 1] = add(top[dz, 1], in_top[dz, 1]).astype(bf16)
        push(top.at[dz, 1], last_top.at[dz], ("last_top", dz), e, ty)
        landed(in_bottom.at[dz], "bottom", dz)
        bottom[dz, 1] = add(bottom[dz, 1], in_bottom[dz, 1]).astype(bf16)
        push(bottom.at[dz, 1], last_bottom.at[dz], ("last_bottom", dz), e, tx)

    def third(dz):
        landed(last_top.at[dz], "last_top", dz)
        landed(last_bottom.at[dz], "last_bottom", dz)
        upper = add(top[dz, 0], in_top[dz, 0], last_top[dz])
        lower = add(bottom[dz, 0], in_bottom[dz, 0], last_bottom[dz])
        if dz:
            share[dz - 1, :half] = upper.astype(bf16)
            share[dz - 1, half:] = lower.astype(bf16)
            copy = pltpu.make_async_remote_copy(
                src_ref=share.at[dz - 1], dst_ref=arrived.at[z], send_sem=sent.at[len(started)],
                recv_sem=got.at[22 * nz + z], device_id={"ep": back(dz) * 2 + c, "tp": t},
                device_id_type=pl.DeviceIdType.MESH)
            copy.start()
            started.append(copy)
        return upper, lower

    def by_width(out, ref, dst):
        right = ref[...].reshape(ep * rows, ref.shape[2])
        for q in range(tp):
            out[pl.ds(q * cols, cols), :] = tn(full[:, 0, q].reshape(ep * rows, cols), right)
        bring(out, dst.at[0])

    spread(1)
    compute(0)
    if nz > 2:
        spread(2)
    for dz in range(1, nz):
        relay(dz)
        if dz + 2 < nz:
            spread(dz + 2)
        if dz > 1:
            second(dz - 2)
        first(dz - 1)
        hand(dz)
        compute(dz)
    for k in range(1, tp):
        push(score, scores.at[t], ("score", k), e, lax.rem(t + k, tp))
    scores[t] = score[...]
    for dz in range(1, nz - 2):
        third(dz)
    second(nz - 2)
    first(nz - 1)
    by_width(g_gate, d_gate, out_gate)
    for dz in range(max(1, nz - 2), nz - 1):
        third(dz)
    second(nz - 1)
    for k in range(1, tp):
        landed(scores.at[lax.rem(t - k + tp, tp)], "score", k)
    total[...] = add(*[scores[j] for j in range(tp)])
    for k in range(1, ep):
        to = lax.rem(e + k, ep)
        push(total.at[to], home.at[e], ("home", k), to, t)
    home[e] = total[e]
    by_width(g_up, d_up, out_up)
    third(nz - 1)
    left = act_w[...].reshape(ep * rows, act_w.shape[2])
    for q in range(tp):
        g_down[:, pl.ds(q * cols, cols)] = tn(left, full[:, 1, q].reshape(ep * rows, cols))
    bring(g_down, out_down.at[0])
    upper, lower = third(0)
    for k in range(1, nz):
        j = lax.rem(z + k, nz)
        pltpu.make_async_remote_copy(
            src_ref=arrived.at[j], dst_ref=arrived.at[j], send_sem=sent.at[0],
            recv_sem=got.at[22 * nz + j], device_id={"ep": side, "tp": t},
            device_id_type=pl.DeviceIdType.MESH).wait_recv()
        upper = upper + arrived[j, :half].astype(f32)
        lower = lower + arrived[j, half:].astype(f32)
    result[:half] = upper.astype(bf16)
    result[half:] = lower.astype(bf16)
    bring(result, out_tok)
    for k in range(1, ep):
        landed(home.at[lax.rem(e - k + ep, ep)], "home", k)
    for j in range(ep):
        out_home[pl.ds(j, 1), :] = home[j, :1]
    assert len(started) <= 20 * nz and len(slots) <= 20 * nz and len(relays) <= 4 * nz
    for copy in started:
        copy.wait_send()
    for go, copy in relays:
        pl.when(go)(copy.wait_send)
    for copy in locals_[len(own) + len(loads):]:
        copy.wait()


def dense(tokens, cotangent, routes, route_weight, w_gate, w_up, w_down):
    f32, bf16 = jnp.float32, jnp.bfloat16
    rows, width = tokens.shape
    ep, tp = lax.axis_size("ep"), lax.axis_size("tp")
    cols, half, nz, hidden = width // tp, rows // 2, ep // 2, w_gate.shape[2]
    hit = routes[None] == jnp.arange(ep, dtype=routes.dtype)[:, None, None]
    table = jnp.sum(jnp.where(hit, route_weight[None], 0.0), axis=2)
    anywhere, near = pl.BlockSpec(memory_space=pltpu.HBM), pl.BlockSpec(memory_space=pltpu.VMEM)
    shape = jax.ShapeDtypeStruct
    grad_tokens, home, gg, gu, gd = pl.pallas_call(
        functools.partial(kernel, ep, tp),
        out_shape=(shape((rows, cols), bf16), shape((ep, rows), f32), shape(w_gate.shape, f32),
                   shape(w_up.shape, f32), shape(w_down.shape, f32)),
        in_specs=[anywhere, anywhere, near, anywhere, anywhere, anywhere],
        out_specs=(anywhere, near, anywhere, anywhere, anywhere),
        scratch_shapes=[
            pltpu.VMEM((ep, 2, tp, rows, cols), bf16),
            pltpu.VMEM((width, hidden), bf16),
            pltpu.VMEM((width, hidden), bf16),
            pltpu.VMEM((hidden, width), bf16),
            pltpu.VMEM((ep, ep, rows), f32),
            pltpu.VMEM((ep, tp, rows, cols), bf16),
            pltpu.VMEM((nz, tp, rows, cols), bf16),
            pltpu.VMEM((nz, 4, half, cols), bf16),
            pltpu.VMEM((nz, 4, half, cols), bf16),
            pltpu.VMEM((nz, 2, half, cols), bf16),
            pltpu.VMEM((nz, 2, half, cols), bf16),
            pltpu.VMEM((nz, half, cols), bf16),
            pltpu.VMEM((nz, half, cols), bf16),
            pltpu.VMEM((nz - 1, rows, cols), bf16),
            pltpu.VMEM((nz, rows, cols), bf16),
            pltpu.VMEM((ep, rows, hidden), bf16),
            pltpu.VMEM((ep, rows, hidden), bf16),
            pltpu.VMEM((ep, rows, hidden), bf16),
            pltpu.VMEM((width, hidden), f32),
            pltpu.VMEM((width, hidden), f32),
            pltpu.VMEM((hidden, width), f32),
            pltpu.VMEM((ep, 8, rows), f32),
            pltpu.VMEM((tp, ep, 8, rows), f32),
            pltpu.VMEM((ep, 8, rows), f32),
            pltpu.VMEM((ep, 8, rows), f32),
            pltpu.VMEM((rows, cols), bf16),
            pltpu.SemaphoreType.DMA((16 + 2 * tp,)),
            pltpu.SemaphoreType.DMA((24 * nz,)),
            pltpu.SemaphoreType.DMA((24 * nz,)),
        ],
        compiler_params=pltpu.CompilerParams(
            collective_id=0, has_side_effects=True, vmem_limit_bytes=50 * 1024 * 1024),
    )(tokens, cotangent, table, w_gate, w_up, w_down)
    grw = jnp.sum(jnp.where(hit, home[:, :, None], 0.0), axis=0)
    return grad_tokens, grw, gg, gu, gd


def on_device(*args):
    rows, width = args[0].shape
    ep, tp = lax.axis_size("ep"), lax.axis_size("tp")
    fits = tp == 4 and ep % 2 == 0 and rows % 128 == 0 and 4 * rows * width * ep <= 1 << 24
    return (dense if fits else slotted)(*args)


def solution(mesh):
    return jax.shard_map(
        on_device,
        mesh=mesh,
        in_specs=(
            P("ep", None),
            P("ep", None),
            P("ep", None),
            P("ep", None),
            P("ep", None, "tp"),
            P("ep", None, "tp"),
            P("ep", "tp", None),
        ),
        out_specs=(
            P("ep", "tp"),
            P("ep", None),
            P("ep", None, "tp"),
            P("ep", None, "tp"),
            P("ep", "tp", None),
        ),
        check_vma=False,
    )
```

profile of v0, /device:TPU:0, one launch (start us, length us, event | category | flops | bytes accessed | tf_op | source)
XLA Modules:
  0.0 90.4 jit_solution(17298228571536511358)
XLA Ops:
  0.6 0.7 select_reduce_fusion.1.table
  1.3 0.0 copy-start
  1.3 1.2 %copy-done = bf16[1,2048,256]{2,1,0:T(8,128)(2,1)S(1)} copy-done((bf16[1,2048,256]{2,1,0:T(8,128)(2,1)S(1)}, bf16[1,2048,256]{2,1,0:T(8,128)(2,1)}, u32[]{:S(2)}) %copy-start) | copy-done | bytes 1048600
  2.6 0.0 copy-start.1
  2.6 1.2 %copy-done.1 = bf16[1,2048,256]{2,1,0:T(8,128)(2,1)S(1)} copy-done((bf16[1,2048,256]{2,1,0:T(8,128)(2,1)S(1)}, bf16[1,2048,256]{2,1,0:T(8,128)(2,1)}, u32[]{:S(2)}) %copy-start.1) | copy-done | bytes 1048600
  3.8 0.0 copy-start.2
  3.8 1.0 %copy-done.2 = bf16[128,2048]{1,0:T(8,128)(2,1)S(1)} copy-done((bf16[128,2048]{1,0:T(8,128)(2,1)S(1)}, bf16[128,2048]{1,0:T(8,128)(2,1)}, u32[]{:S(2)}) %copy-start.2) | copy-done | bytes 524312
  4.8 0.0 copy-start.3
  4.8 1.0 %copy-done.3 = bf16[128,2048]{1,0:T(8,128)(2,1)S(1)} copy-done((bf16[128,2048]{1,0:T(8,128)(2,1)S(1)}, bf16[128,2048]{1,0:T(8,128)(2,1)}, u32[]{:S(2)}) %copy-start.3) | copy-done | bytes 524312
  5.9 0.0 copy-start.6
  5.9 76.5 %shard_map.110 = (bf16[128,512]{1,0:T(8,128)(2,1)S(1)}, f32[8,128]{1,0:T(8,128)S(1)}, f32[1,2048,256]{2,1,0:T(8,128)}, f32[1,2048,256]{2,1,0:T(8,128)}, f32[1,256,2048]{2,1,0:T(8,128)}) custom-call(bf16[128,2048]{1,0:T(8,128)(2,1)S(1)} %copy-done.2, bf16[128,2048]{1,0:T(8,128)(2,1)S(1)} %copy-done.3, f32[8,128]{1,0:T(8,128)S(1)} %select_reduce_fusion.1.table, ...), custom_call_target="tpu_custom_call" | custom-call | tf_op jit(solution)/shard_map/pallas_call | solution.py:389
  82.3 0.0 copy-done.6
  82.3 0.6 select_reduce_fusion
  82.9 0.7 copy.18
  83.6 0.0 copy-start.5
  83.6 3.2 %copy.19 = f32[1,2048,256]{2,1,0:T(8,128)} copy(f32[1,2048,256]{2,1,0:T(8,128)} %get-tuple-element.22) | data formatting | bytes 4194304
  86.8 0.0 copy-done.5
  86.8 0.0 copy-start.4
  86.8 1.3 %copy.20 = f32[1,2048,256]{2,1,0:T(8,128)} copy(f32[1,2048,256]{2,1,0:T(8,128)S(1)} %copy-done.5) | data formatting | bytes 4194304
  88.1 1.0 %copy-done.4 = f32[1,256,2048]{2,1,0:T(8,128)S(1)} copy-done((f32[1,256,2048]{2,1,0:T(8,128)S(1)}, f32[1,256,2048]{2,1,0:T(8,128)}, u32[]{:S(2)}) %copy-start.4) | copy-done | bytes 2097176
  89.1 1.3 %copy.21 = f32[1,256,2048]{2,1,0:T(8,128)} copy(f32[1,256,2048]{2,1,0:T(8,128)S(1)} %copy-done.4) | data formatting | bytes 4194304
Async XLA Ops:
  1.3 1.2 %copy-start = (bf16[1,2048,256]{2,1,0:T(8,128)(2,1)S(1)}, bf16[1,2048,256]{2,1,0:T(8,128)(2,1)}, u32[]{:S(2)}) copy-start(bf16[1,2048,256]{2,1,0:T(8,128)(2,1)} %w_gate.1) | copy-start | bytes 3145732
  2.6 1.2 %copy-start.1 = (bf16[1,2048,256]{2,1,0:T(8,128)(2,1)S(1)}, bf16[1,2048,256]{2,1,0:T(8,128)(2,1)}, u32[]{:S(2)}) copy-start(bf16[1,2048,256]{2,1,0:T(8,128)(2,1)} %w_up.1) | copy-start | bytes 3145732
  3.8 1.0 %copy-start.2 = (bf16[128,2048]{1,0:T(8,128)(2,1)S(1)}, bf16[128,2048]{1,0:T(8,128)(2,1)}, u32[]{:S(2)}) copy-start(bf16[128,2048]{1,0:T(8,128)(2,1)} %tokens.1) | copy-start | bytes 1572868
  4.8 1.0 %copy-start.3 = (bf16[128,2048]{1,0:T(8,128)(2,1)S(1)}, bf16[128,2048]{1,0:T(8,128)(2,1)}, u32[]{:S(2)}) copy-start(bf16[128,2048]{1,0:T(8,128)(2,1)} %cotangent.1) | copy-start | bytes 1572868
  5.9 76.5 %copy-start.6 = (s32[128,2]{0,1:T(2,128)S(1)}, s32[128,2]{0,1:T(2,128)}, u32[]{:S(2)}) copy-start(s32[128,2]{0,1:T(2,128)} %param.9) | copy-start | bytes 3076
  83.6 3.2 %copy-start.5 = (f32[1,2048,256]{2,1,0:T(8,128)S(1)}, f32[1,2048,256]{2,1,0:T(8,128)}, u32[]{:S(2)}) copy-start(f32[1,2048,256]{2,1,0:T(8,128)} %get-tuple-element.23) | copy-start | bytes 6291460
  86.8 2.3 %copy-start.4 = (f32[1,256,2048]{2,1,0:T(8,128)S(1)}, f32[1,256,2048]{2,1,0:T(8,128)}, u32[]{:S(2)}) copy-start(f32[1,256,2048]{2,1,0:T(8,128)} %get-tuple-element.24) | copy-start | bytes 6291460
where the time goes:
time: 90.8 us; the launch traced here: 90.4 us
  Pallas kernels  76.5 us (84%)
  local copies, waits for them, and re-layouts  12.1 us (13%)
  other arithmetic  1.28 us (1%)
    pallas_call x1, Pallas kernels, dense(): pl.pallas_call(functools.partial(kernel, ep, tp), out_shape=(shape((rows,...  76.5 us
    unnamed x18, local copies, waits for them, and re-layouts  12.1 us

commit v1 on v0

--- a/solution.py
+++ b/solution.py
@@ -104,11 +104,11 @@
     return (grad_tokens, grad_route_weight, grad_gate, grad_up, grad_down)
 
 
-def kernel(ep, tp, tokens, cotangent, table, w_gate, w_up, w_down,
-           out_tok, out_home, out_gate, out_up, out_down,
+def kernel(ep, tp, tokens, cotangent, routes, route_weight, w_gate, w_up, w_down,
+           result, out_home, g_gate, g_up, g_down,
            full, gate_v, up_v, down_v, weights, part, other, top, bottom,
            in_top, in_bottom, last_top, last_bottom, share, arrived,
-           d_gate, d_up, act_w, g_gate, g_up, g_down, score, scores, total, home, result,
+           d_gate, d_up, act_w, table, score, scores, total, home,
            local, sent, got):
     f32, bf16 = jnp.float32, jnp.bfloat16
     rows, width = tokens.shape
@@ -147,6 +147,9 @@
     own = [bring(ref.at[:, pl.ds(q * cols, cols)], full.at[e, a, q])
            for a, ref in enumerate((tokens, cotangent)) for q in range(tp)]
     loads = [bring(w_gate.at[0], gate_v), bring(w_up.at[0], up_v), bring(w_down.at[0], down_v)]
+    named = lax.broadcasted_iota(jnp.int32, (ep, rows), 0)
+    hits = [named == routes[pl.ds(k, 1), :] for k in range(routes.shape[0])]
+    table[...] = sum(jnp.where(hit, route_weight[pl.ds(k, 1), :], 0.0) for k, hit in enumerate(hits))
     weights[e] = table[...]
 
     barrier = pltpu.get_barrier_semaphore()
@@ -309,11 +312,10 @@
             started.append(copy)
         return upper, lower
 
-    def by_width(out, ref, dst):
+    def by_width(out, ref):
         right = ref[...].reshape(ep * rows, ref.shape[2])
         for q in range(tp):
-            out[pl.ds(q * cols, cols), :] = tn(full[:, 0, q].reshape(ep * rows, cols), right)
-        bring(out, dst.at[0])
+            out[0, pl.ds(q * cols, cols), :] = tn(full[:, 0, q].reshape(ep * rows, cols), right)
 
     spread(1)
     compute(0)
@@ -335,7 +337,7 @@
         third(dz)
     second(nz - 2)
     first(nz - 1)
-    by_width(g_gate, d_gate, out_gate)
+    by_width(g_gate, d_gate)
     for dz in range(max(1, nz - 2), nz - 1):
         third(dz)
     second(nz - 1)
@@ -346,12 +348,11 @@
         to = lax.rem(e + k, ep)
         push(total.at[to], home.at[e], ("home", k), to, t)
     home[e] = total[e]
-    by_width(g_up, d_up, out_up)
+    by_width(g_up, d_up)
     third(nz - 1)
     left = act_w[...].reshape(ep * rows, act_w.shape[2])
     for q in range(tp):
-        g_down[:, pl.ds(q * cols, cols)] = tn(left, full[:, 1, q].reshape(ep * rows, cols))
-    bring(g_down, out_down.at[0])
+        g_down[0, :, pl.ds(q * cols, cols)] = tn(left, full[:, 1, q].reshape(ep * rows, cols))
     upper, lower = third(0)
     for k in range(1, nz):
         j = lax.rem(z + k, nz)
@@ -363,17 +364,25 @@
         lower = lower + arrived[j, half:].astype(f32)
     result[:half] = upper.astype(bf16)
     result[half:] = lower.astype(bf16)
-    bring(result, out_tok)
     for k in range(1, ep):
         landed(home.at[lax.rem(e - k + ep, ep)], "home", k)
-    for j in range(ep):
-        out_home[pl.ds(j, 1), :] = home[j, :1]
+    back_home = jnp.concatenate([home[j, :1] for j in range(ep)], axis=0)
+    for k, hit in enumerate(hits):
+        out_home[pl.ds(k, 1), :] = jnp.sum(jnp.where(hit, back_home, 0.0), axis=0, keepdims=True)
     assert len(started) <= 20 * nz and len(slots) <= 20 * nz and len(relays) <= 4 * nz
     for copy in started:
         copy.wait_send()
     for go, copy in relays:
         pl.when(go)(copy.wait_send)
-    for copy in locals_[len(own) + len(loads):]:
+
+
+def deliver(*refs):
+    half = (len(refs) - 1) // 2
+    copies = [pltpu.make_async_copy(src, dst, refs[-1].at[i])
+              for i, (src, dst) in enumerate(zip(refs[:half], refs[half:-1]))]
+    for copy in copies:
+        copy.start()
+    for copy in copies:
         copy.wait()
 
 
@@ -382,16 +391,17 @@
     rows, width = tokens.shape
     ep, tp = lax.axis_size("ep"), lax.axis_size("tp")
     cols, half, nz, hidden = width // tp, rows // 2, ep // 2, w_gate.shape[2]
-    hit = routes[None] == jnp.arange(ep, dtype=routes.dtype)[:, None, None]
-    table = jnp.sum(jnp.where(hit, route_weight[None], 0.0), axis=2)
     anywhere, near = pl.BlockSpec(memory_space=pltpu.HBM), pl.BlockSpec(memory_space=pltpu.VMEM)
-    shape = jax.ShapeDtypeStruct
-    grad_tokens, home, gg, gu, gd = pl.pallas_call(
+
+    def held(space, *arrays):
+        return [pltpu.with_memory_space_constraint(x, space) for x in arrays]
+
+    shapes = ((rows, cols), bf16), (routes.T.shape, f32), (w_gate.shape, f32), (w_up.shape, f32), (w_down.shape, f32)
+    parts = pl.pallas_call(
         functools.partial(kernel, ep, tp),
-        out_shape=(shape((rows, cols), bf16), shape((ep, rows), f32), shape(w_gate.shape, f32),
-                   shape(w_up.shape, f32), shape(w_down.shape, f32)),
-        in_specs=[anywhere, anywhere, near, anywhere, anywhere, anywhere],
-        out_specs=(anywhere, near, anywhere, anywhere, anywhere),
+        out_shape=tuple(pltpu.VMEM(*shape) for shape in shapes),
+        in_specs=[anywhere, anywhere, near, near, anywhere, anywhere, anywhere],
+        out_specs=(near,) * 5,
         scratch_shapes=[
             pltpu.VMEM((ep, 2, tp, rows, cols), bf16),
             pltpu.VMEM((width, hidden), bf16),
@@ -411,23 +421,28 @@
             pltpu.VMEM((ep, rows, hidden), bf16),
             pltpu.VMEM((ep, rows, hidden), bf16),
             pltpu.VMEM((ep, rows, hidden), bf16),
-            pltpu.VMEM((width, hidden), f32),
-            pltpu.VMEM((width, hidden), f32),
-            pltpu.VMEM((hidden, width), f32),
+            pltpu.VMEM((ep, rows), f32),
             pltpu.VMEM((ep, 8, rows), f32),
             pltpu.VMEM((tp, ep, 8, rows), f32),
             pltpu.VMEM((ep, 8, rows), f32),
             pltpu.VMEM((ep, 8, rows), f32),
-            pltpu.VMEM((rows, cols), bf16),
             pltpu.SemaphoreType.DMA((16 + 2 * tp,)),
             pltpu.SemaphoreType.DMA((24 * nz,)),
             pltpu.SemaphoreType.DMA((24 * nz,)),
         ],
         compiler_params=pltpu.CompilerParams(
             collective_id=0, has_side_effects=True, vmem_limit_bytes=50 * 1024 * 1024),
-    )(tokens, cotangent, table, w_gate, w_up, w_down)
-    grw = jnp.sum(jnp.where(hit, home[:, :, None], 0.0), axis=0)
-    return grad_tokens, grw, gg, gu, gd
+    )(*held(pltpu.HBM, tokens, cotangent), routes.T, route_weight.T,
+      *held(pltpu.HBM, w_gate, w_up, w_down))
+    grad_tokens, grw, *grads = pl.pallas_call(
+        deliver,
+        out_shape=tuple(jax.ShapeDtypeStruct(*shape) for shape in shapes),
+        in_specs=[near] * 5,
+        out_specs=(anywhere,) * 5,
+        scratch_shapes=[pltpu.SemaphoreType.DMA((5,))],
+        compiler_params=pltpu.CompilerParams(vmem_limit_bytes=1 << 20),
+    )(*held(pltpu.VMEM, *parts))
+    return grad_tokens, grw.T, *grads
 
 
 def on_device(*args):

time: 90.8 us -> 80.3 us (0.88)
  local copies, waits for them, and re-layouts: 12.1 us -> 0 us
  Pallas kernels: 76.5 us -> 79.5 us
  other arithmetic: 1.28 us -> 0 us
    unnamed x18 -> x0, local copies, waits for them, and re-layouts: 12.1 us -> none
    pallas_call x1 -> x2, Pallas kernels: 76.5 us -> 79.5 us  [the longest x1 76.7 us: dense(): pl.pallas_call(functools.partial(kernel, ep, tp), out_shape=tuple((pltpu....]
    reduce_sum x2 -> x0, other arithmetic: 1.28 us -> none  [the longest x1 0.7 us: dense(): table = jnp.sum(jnp.where(hit, route_weight[None], 0.0), axis=2)]
where the time goes in v1:
time: 80.3 us; the launch traced here: 80.1 us
  Pallas kernels  79.5 us (99%)
    pallas_call x1, Pallas kernels, dense(): pl.pallas_call(functools.partial(kernel, ep, tp), out_shape=tuple((pltpu....  76.7 us
    pallas_call x1, Pallas kernels, dense(): pl.pallas_call(deliver, out_shape=tuple((jax.ShapeDtypeStruct(*shape) for...  2.79 us

profile of v1, /device:TPU:0, one launch (start us, length us, event | category | flops | bytes accessed | tf_op | source)
XLA Modules:
  0.0 80.1 jit_solution(11004672818937044661)
XLA Ops:
  0.6 76.7 %shard_map.110 = (bf16[128,512]{1,0:T(8,128)(2,1)S(1)}, f32[2,128]{1,0:T(2,128)S(1)}, f32[1,2048,256]{2,1,0:T(8,128)S(1)}, f32[1,2048,256]{2,1,0:T(8,128)S(1)}, f32[1,256,2048]{2,1,0:T(8,128)S(1)}) custom-call(bf16[128,2048]{1,0:T(8,128)(2,1)} %tokens.1, bf16[128,2048]{1,0:T(8,128)(2,1)} %cotangent.1, s32[2,128]{1,0:T(2,128)} %bitcast.3, f32[2,128]{1,0:T(2,128)} %bitcast.4, ...), custom_call_target="tpu_custom_call" | custom-call | tf_op jit(solution)/shard_map/pallas_call | solution.py:400
  77.3 2.8 %shard_map.111 = (bf16[128,512]{1,0:T(8,128)(2,1)}, f32[2,128]{1,0:T(2,128)}, f32[1,2048,256]{2,1,0:T(8,128)}, f32[1,2048,256]{2,1,0:T(8,128)}, f32[1,256,2048]{2,1,0:T(8,128)}) custom-call(bf16[128,512]{1,0:T(8,128)(2,1)S(1)} %get-tuple-element.15.refs_0_, f32[2,128]{1,0:T(2,128)S(1)} %get-tuple-element.16.refs_1_, ...), custom_call_target="tpu_custom_call" | custom-call | tf_op jit(solution)/shard_map/pallas_call | solution.py:437

commit v2 on v1

v2 whole, which is shorter than its diff:
```python
import functools

import jax
import jax.numpy as jnp
from jax import lax
from jax.experimental import pallas as pl
from jax.experimental.pallas import tpu as pltpu
from jax.sharding import PartitionSpec as P


def slot_index(block_routes, experts, capacity):
    flat_ids = block_routes.reshape(-1)
    onehot = (flat_ids[:, None] == jnp.arange(experts, dtype=jnp.int32)[None, :]).astype(jnp.int32)
    earlier = jnp.cumsum(onehot, axis=0) - onehot
    return flat_ids * capacity + jnp.sum(earlier * onehot, axis=1)


def slotted(tokens, cotangent, routes, route_weight, w_gate, w_up, w_down):
    f32 = jnp.float32
    tok_rows, model_width = tokens.shape
    choices_row = routes.shape[1]
    experts = lax.axis_size("ep")
    capacity = 2 * tok_rows * choices_row // experts
    recv_rows = experts * capacity
    slot_ids = slot_index(routes, experts, capacity)
    send_w = jnp.zeros((recv_rows,), f32).at[slot_ids].set(route_weight.reshape(-1))
    send_x = (
        jnp.zeros((recv_rows, model_width), jnp.bfloat16)
        .at[slot_ids]
        .set(jnp.repeat(tokens, choices_row, axis=0))
    )
    send_dy = (
        jnp.zeros((recv_rows, model_width), jnp.bfloat16)
        .at[slot_ids]
        .set(jnp.repeat(cotangent, choices_row, axis=0))
    )
    got_x = lax.all_to_all(
        send_x.reshape(experts, capacity, model_width),
        "ep",
        split_axis=0,
        concat_axis=0,
        tiled=True,
    )
    got_dy, got_w = (
        lax.all_to_all(
            send_dy.reshape(experts, capacity, model_width),
            "ep",
            split_axis=0,
            concat_axis=0,
            tiled=True,
        ),
        lax.all_to_all(
            send_w.reshape(experts, capacity, 1).astype(jnp.bfloat16),
            "ep",
            split_axis=0,
            concat_axis=0,
            tiled=True,
        ).astype(jnp.float32),
    )
    rows_x = got_x.reshape(recv_rows, model_width)
    rows_dy = got_dy.reshape(recv_rows, model_width)
    rows_w = got_w.reshape(recv_rows)
    gate_w = w_gate[0]
    up_w = w_up[0]
    down_w = w_down[0]
    gate_pre = jnp.dot(rows_x, gate_w, preferred_element_type=f32)
    up_pre = jnp.dot(rows_x, up_w, preferred_element_type=f32)
    gate_sig = jax.nn.sigmoid(gate_pre)
    act_full = gate_pre * gate_sig * up_pre
    act = act_full.astype(jnp.bfloat16)
    back_hidden = jnp.einsum("rd,fd->rf", rows_dy, down_w, preferred_element_type=f32)
    weighted_cot = (rows_w[:, None] * rows_dy.astype(f32)).astype(jnp.bfloat16)
    d_hidden = rows_w[:, None] * back_hidden
    d_gate = (d_hidden * up_pre * gate_sig * (1.0 + gate_pre * (1.0 - gate_sig))).astype(
        jnp.bfloat16
    )
    d_up = (d_hidden * gate_pre * gate_sig).astype(jnp.bfloat16)
    gate_part = jnp.sum(act_full * back_hidden, axis=1)
    token_part = jnp.einsum("rf,df->rd", d_gate, gate_w, preferred_element_type=f32)
    token_part = token_part + jnp.einsum("rf,df->rd", d_up, up_w, preferred_element_type=f32)
    grad_gate = jnp.einsum("rd,rf->df", rows_x, d_gate, preferred_element_type=f32)[None]
    grad_up = jnp.einsum("rd,rf->df", rows_x, d_up, preferred_element_type=f32)[None]
    grad_down = jnp.einsum("rf,rd->fd", act, weighted_cot, preferred_element_type=f32)[None]
    rounded_part = token_part.astype(jnp.bfloat16).astype(f32)
    shares = lax.psum_scatter(
        rounded_part.astype(jnp.bfloat16), "tp", scatter_dimension=1, tiled=True
    )
    gate_total = lax.psum(gate_part, "tp")
    back_x, back_gate = (
        lax.all_to_all(
            shares.reshape(experts, capacity, -1), "ep", split_axis=0, concat_axis=0, tiled=True
        ),
        lax.all_to_all(
            gate_total.reshape(experts, capacity).astype(jnp.bfloat16),
            "ep",
            split_axis=0,
            concat_axis=0,
            tiled=True,
        ).astype(jnp.float32),
    )
    picked = back_x.reshape(recv_rows, -1)[slot_ids].astype(f32).reshape(tok_rows, choices_row, -1)
    grad_route_weight = back_gate.reshape(recv_rows)[slot_ids].reshape(tok_rows, choices_row)
    grad_tokens = jnp.sum(picked, axis=1).astype(jnp.bfloat16)
    return (grad_tokens, grad_route_weight, grad_gate, grad_up, grad_down)


def kernel(ep, tp, tokens, cotangent, routes, route_weight, w_gate, w_up, w_down,
           result, out_home, g_gate, g_up, g_down,
           full, gate_v, up_v, down_v, weights, part, other, top, bottom,
           in_top, in_bottom, last_top, last_bottom, share, arrived,
           d_gate, d_up, act_w, score, score_rows, scores, total, home,
           local, sent, got):
    f32, bf16 = jnp.float32, jnp.bfloat16
    rows, width = tokens.shape
    cols = width // tp
    half = rows // 2
    nz = ep // 2
    e, t = lax.axis_index("ep"), lax.axis_index("tp")
    z, c = e // 2, lax.rem(e, 2)
    y, x = t // 2, lax.rem(t, 2)
    side = z * 2 + 1 - c
    tx, ty = y * 2 + 1 - x, (1 - y) * 2 + x
    td = (1 - y) * 2 + 1 - x
    onward = jnp.where(z < nz // 2, 1, -1)
    middle = jnp.logical_and(z > 0, z < nz - 1)
    outer = jnp.logical_not(middle)
    lead = jnp.where(middle, onward, 0)
    back = [z, z + onward - 2 * lead, z + 2 * onward, z + 3 * onward - 2 * lead]
    behind, ahead = z + onward - 2 * lead, z + onward
    names = {}
    groups = {"pair": 0, "plane": 1, "side": 2, "own": 3, "halves": 4, "quarters": 5, "home": 6, "small": 7,
              "relay": 8, "relay_w": 9}

    def scope(name):
        return jax.named_scope(name)

    def slot(name, count=1):
        if name not in names:
            names[name] = sum(n for _, n in names.values()), count
        return names[name][0]

    def plan(group, src, dst, slot_at, to_e, to_t):
        return pltpu.make_async_remote_copy(
            src_ref=src, dst_ref=dst, send_sem=sent.at[groups[group]], recv_sem=got.at[slot_at],
            device_id={"ep": to_e, "tp": to_t}, device_id_type=pl.DeviceIdType.MESH)

    def push(*args):
        plan(*args).start()

    def drained(group, ref):
        pltpu.make_async_remote_copy(
            src_ref=ref, dst_ref=ref, send_sem=sent.at[groups[group]], recv_sem=got.at[0],
            device_id={"ep": side, "tp": t}, device_id_type=pl.DeviceIdType.MESH).wait_send()

    def landing(dst, slot_at):
        return pltpu.make_async_remote_copy(
            src_ref=dst, dst_ref=dst, send_sem=sent.at[0], recv_sem=got.at[slot_at],
            device_id={"ep": side, "tp": t}, device_id_type=pl.DeviceIdType.MESH)

    def landed(dst, slot_at, label="w"):
        with scope(label):
            landing(dst, slot_at).wait_recv()

    own = [pltpu.make_async_copy(ref.at[:, pl.ds(q * cols, cols)], full.at[e, a, q], local.at[0])
           for a, ref in enumerate((tokens, cotangent)) for q in range(tp)]
    loads = [pltpu.make_async_copy(src.at[0], dst, local.at[1 + i])
             for i, (src, dst) in enumerate(((w_gate, gate_v), (w_up, up_v), (w_down, down_v)))]
    for copy in own + loads:
        copy.start()
    slot("along", 4 * nz), slot("x", 2 * nz - 2), slot("y", 2 * nz - 2), slot("dx", nz - 1), slot("dy", nz - 1)
    slot("side", nz), slot("side_w", nz), slot("pair", 3 * nz), slot("top", nz), slot("bottom", nz)
    slot("last_top", nz), slot("last_bottom", nz), slot("share"), slot("score"), slot("home")

    barrier = pltpu.get_barrier_semaphore()

    def greet(to_e, to_t):
        pl.semaphore_signal(barrier, inc=1, device_id={"ep": to_e, "tp": to_t},
                            device_id_type=pl.DeviceIdType.MESH)

    greet(side, t)
    greet(e, tx)
    greet(e, ty)
    greet(ahead * 2 + c, t)
    pl.when(middle)(lambda: greet(behind * 2 + c, t))

    named = lax.broadcasted_iota(jnp.int32, (ep, rows), 0)
    hits = [named == routes[pl.ds(k, 1), :] for k in range(routes.shape[0])]
    weights[e] = sum(jnp.where(hit, route_weight[pl.ds(k, 1), :], 0.0) for k, hit in enumerate(hits))

    with scope("own"):
        pltpu.make_async_copy(full.at[e], full.at[e], local.at[0]).wait()
    with scope("barrier"):
        pl.semaphore_wait(barrier, jnp.where(middle, 5, 4))

    def pieces(s):
        return full.at[s, 0, t], full.at[s, 1, t], full.at[s, 1, td], weights.at[s]

    def along(block, k):
        return slot("along") + block * 4 + k

    for k, piece in enumerate(pieces(e)):
        push("small" if k == 3 else "own", piece, piece, along(z, k), ahead * 2 + c, t)
        copy = plan("relay_w" if k == 3 else "relay", piece, piece, along(z, k), behind * 2 + c, t)
        pl.when(middle)(copy.start)
    push("small", weights.at[e], weights.at[e], slot("side_w"), side, t)
    push("side", full.at[e], full.at[e], slot("side"), side, t)

    def step(dz, k, onto, only=None):
        block = back[dz]
        piece = pieces(block * 2 + c)[k]
        arrival = landing(piece, along(block, k))
        if only is not outer:
            passed = plan("relay_w" if k == 3 else "relay", piece, piece, along(block, k), onto * 2 + c, t)
        copies = []
        if k < 2:
            copies.append(plan("plane", piece, piece, slot("x") + dz * 2 - 2 + k, e, tx))
            copies.append(plan("plane", piece, piece, slot("y") + dz * 2 - 2 + k, e, ty))
        if k == 3:
            copies.append(plan("small", piece, piece, slot("side_w") + dz, side, t))
        else:
            copies.append(plan("side", piece, piece, slot("side") + dz, side, t))

        def run():
            arrival.wait_recv()
            if only is None:
                pl.when(middle)(passed.start)
            elif only is middle:
                passed.start()
            for copy in copies:
                copy.start()

        with scope(f"z{k}_{dz}{'' if only is None else 'm' if only is middle else 'o'}"):
            run() if only is None else pl.when(only)(run)

    def near(k):
        step(1, k, ahead)
        step(3, k, behind, middle)

    def far(k):
        step(2, k, behind)

    def last(k):
        step(3, k, behind, outer)

    def aside(dz, a, q):
        piece = full.at[back[dz] * 2 + c, a, q]
        push("side", piece, piece, slot("side") + dz, side, t)

    def relay(dz):
        s = back[dz] * 2 + c
        landed(full.at[s, 0, ty], slot("y") + dz * 2 - 2, f"y0_{dz}")
        piece = full.at[s, 0, ty, :half]
        push("quarters", piece, piece, slot("dx") + dz - 1, e, tx)
        landed(full.at[s, 0, tx], slot("x") + dz * 2 - 2, f"x0_{dz}")
        piece = full.at[s, 0, tx, half:]
        push("quarters", piece, piece, slot("dy") + dz - 1, e, ty)
        aside(dz, 0, ty)
        aside(dz, 0, tx)

    def crossed(dz):
        s = back[dz] * 2 + c
        landed(full.at[s, 1, ty], slot("y") + dz * 2 - 1, f"y1_{dz}")
        aside(dz, 1, ty)
        landed(full.at[s, 1, tx], slot("x") + dz * 2 - 1, f"x1_{dz}")
        aside(dz, 1, tx)

    def diagonal(dz):
        s = back[dz] * 2 + c
        landed(full.at[s, 0, td, :half], slot("dx") + dz - 1, f"dx_{dz}")
        landed(full.at[s, 0, td, half:], slot("dy") + dz - 1, f"dy_{dz}")
        aside(dz, 0, td)

    def nt(a, b):
        return lax.dot_general(a, b, (((1,), (1,)), ((), ())), preferred_element_type=f32)

    def tn(a, b):
        return lax.dot_general(a, b, (((0,), (0,)), ((), ())), preferred_element_type=f32)

    def column(block):
        mine = lax.broadcasted_iota(jnp.int32, (ep, rows), 0) == e
        row = jnp.sum(jnp.where(mine, weights[block], 0.0), axis=0, keepdims=True)
        return jnp.transpose(jnp.broadcast_to(row, (rows, rows)))[:, :1]

    def forward(dz):
        b = back[dz] * 2
        landed(full.at[b + 1 - c], slot("side") + dz, f"side_{dz}")
        landed(weights.at[b + 1 - c], slot("side_w") + dz, f"sidew_{dz}")
        with scope(f"fwd_{dz}"):
            g = u = bk = None
            for q in range(tp):
                span = pl.ds(q * cols, cols)
                xs = jnp.concatenate([full[b, 0, q], full[b + 1, 0, q]], axis=0)
                dy = jnp.concatenate([full[b, 1, q], full[b + 1, 1, q]], axis=0)
                g_q = jnp.dot(xs, gate_v[span, :], preferred_element_type=f32)
                u_q = jnp.dot(xs, up_v[span, :], preferred_element_type=f32)
                b_q = nt(dy, down_v[:, span])
                g, u, bk = (g_q, u_q, b_q) if q == 0 else (g + g_q, u + u_q, bk + b_q)
            w = jnp.concatenate([column(b), column(b + 1)], axis=0)
            sig = jax.nn.sigmoid(g)
            silu = g * sig
            act = silu * u
            d_h = w * bk
            dg = (d_h * u * sig * (1.0 + g * (1.0 - sig))).astype(bf16)
            du = (d_h * silu).astype(bf16)
            aw = (w * act).astype(bf16)
            sums = jnp.sum(act * bk, axis=1, keepdims=True)
            for i in range(2):
                cut = slice(i * rows, (i + 1) * rows)
                d_gate[b + i] = dg[cut]
                d_up[b + i] = du[cut]
                act_w[b + i] = aw[cut]
                score[b + i] = jnp.transpose(jnp.broadcast_to(sums[cut], (rows, rows)))[:8]

    def backward(dz):
        b = back[dz] * 2
        with scope(f"bwd_{dz}"):
            dg = jnp.concatenate([d_gate[b], d_gate[b + 1]], axis=0)
            du = jnp.concatenate([d_up[b], d_up[b + 1]], axis=0)
            for r, q in enumerate((td, tx, ty, t)):
                span = pl.ds(pl.multiple_of(q * cols, cols), cols)
                piece = (nt(dg, gate_v[span, :]) + nt(du, up_v[span, :])).astype(bf16)
                part[b, q] = piece[:rows]
                part[b + 1, q] = piece[rows:]
                push("pair", part.at[b + 1 - c, q], other.at[dz, q], slot("pair") + dz * 3 + max(r - 1, 0), side, t)

    def add(*terms):
        value = terms[0].astype(f32)
        for term in terms[1:]:
            value = value + term.astype(f32)
        return value

    def first(dz):
        s = back[dz] * 2 + c

        def both(q, upper):
            cut = slice(0, half) if upper else slice(half, rows)
            return add(part[s, q, cut], other[dz, q, cut]).astype(bf16)

        landed(other.at[dz, pl.ds(0, 2)], slot("pair") + dz * 3, f"pair0_{dz}")
        top[dz, 3] = both(td, True)
        top[dz, 2] = both(tx, True)
        push("halves", top.at[dz, pl.ds(2, 2)], in_top.at[dz], slot("top") + dz, e, tx)
        landed(other.at[dz, ty], slot("pair") + dz * 3 + 1, f"pair2_{dz}")
        bottom[dz, 3] = both(td, False)
        bottom[dz, 2] = both(ty, False)
        push("halves", bottom.at[dz, pl.ds(2, 2)], in_bottom.at[dz], slot("bottom") + dz, e, ty)
        landed(other.at[dz, t], slot("pair") + dz * 3 + 2, f"pair3_{dz}")
        top[dz, 0] = both(t, True)
        top[dz, 1] = both(ty, True)
        bottom[dz, 0] = both(t, False)
        bottom[dz, 1] = both(tx, False)

    def second(dz):
        landed(in_top.at[dz], slot("top") + dz, f"top_{dz}")
        top[dz, 1] = add(top[dz, 1], in_top[dz, 1]).astype(bf16)
        push("quarters", top.at[dz, 1], last_top.at[dz], slot("last_top") + dz, e, ty)
        landed(in_bottom.at[dz], slot("bottom") + dz, f"bottom_{dz}")
        bottom[dz, 1] = add(bottom[dz, 1], in_bottom[dz, 1]).astype(bf16)
        push("quarters", bottom.at[dz, 1], last_bottom.at[dz], slot("last_bottom") + dz, e, tx)

    def third(dz):
        halves = []
        for cut, mine, got_in, ending, name in (
                (pl.ds(0, half), top, in_top, last_top, "last_top"),
                (pl.ds(half, half), bottom, in_bottom, last_bottom, "last_bottom")):
            landed(ending.at[dz], slot(name) + dz, f"{name}_{dz}")
            value = add(mine[dz, 0], got_in[dz, 0], ending[dz])
            if dz:
                share[dz - 1, cut] = value.astype(bf16)
                push("quarters", share.at[dz - 1, cut], arrived.at[z, cut], slot("share"), back[dz] * 2 + c, t)
            halves.append(value)
        return halves

    def by_width(out, ref, name):
        with scope(name):
            right = ref[...].reshape(ep * rows, ref.shape[2])
            for q in range(tp):
                out[0, pl.ds(q * cols, cols), :] = tn(full[:, 0, q].reshape(ep * rows, cols), right)

    with scope("loads"):
        for copy in loads:
            copy.wait()
    forward(0)
    near(0)
    backward(0)
    near(1)
    first(0)
    relay(1)
    near(2)
    near(3)
    crossed(1)
    far(0)
    diagonal(1)
    second(0)
    forward(1)
    far(1)
    backward(1)
    relay(2)
    first(1)
    far(2)
    far(3)
    crossed(2)
    last(0)
    diagonal(2)
    forward(2)
    last(1)
    backward(2)
    second(1)
    relay(3)
    last(2)
    last(3)
    first(2)
    crossed(3)
    third(1)
    diagonal(3)
    forward(3)
    backward(3)
    second(2)
    score_rows[...] = jnp.concatenate([score[j, :1] for j in range(ep)], axis=0)
    for k in range(1, tp):
        push("small", score_rows, scores.at[t], slot("score"), e, lax.rem(t + k, tp))
    scores[t] = score_rows[...]
    third(2)
    first(3)
    by_width(g_gate, d_gate, "wg_gate")
    landed(scores.at[pl.ds(0, tp - 1)], slot("score"), "score")
    total[...] = add(*[scores[j] for j in range(tp)])
    for k in range(1, ep):
        push("home", total, home.at[e], slot("home"), lax.rem(e + k, ep), t)
    home[e] = total[...]
    by_width(g_up, d_up, "wg_up")
    second(3)
    with scope("wg_down"):
        left = act_w[...].reshape(ep * rows, act_w.shape[2])
        for q in range(tp):
            g_down[0, :, pl.ds(q * cols, cols)] = tn(left, full[:, 1, q].reshape(ep * rows, cols))
    third(3)
    upper, lower = third(0)
    landed(arrived.at[pl.ds(0, nz - 1)], slot("share"), "arrived")
    for k in range(1, nz):
        j = lax.rem(z + k, nz)
        upper = upper + arrived[j, :half].astype(f32)
        lower = lower + arrived[j, half:].astype(f32)
    result[:half] = upper.astype(bf16)
    result[half:] = lower.astype(bf16)
    landed(home.at[pl.ds(0, ep - 1)], slot("home"), "home")
    back_home = jnp.concatenate(
        [jnp.sum(jnp.where(named == e, home[j], 0.0), axis=0, keepdims=True) for j in range(ep)], axis=0)
    for k, hit in enumerate(hits):
        out_home[pl.ds(k, 1), :] = jnp.sum(jnp.where(hit, back_home, 0.0), axis=0, keepdims=True)
    assert sum(n for _, n in names.values()) == got.shape[0]
    with scope("final"):
        drained("pair", other)
        drained("plane", full.at[pl.ds(0, 3), 0])
        drained("side", full.at[pl.ds(0, 4)])
        drained("own", full.at[0, 0, pl.ds(0, 3)])
        drained("halves", full.at[0])
        drained("quarters", full.at[pl.ds(0, 5), 0, pl.ds(0, 2)])
        drained("home", weights.at[pl.ds(0, ep - 1)])
        drained("small", weights)

        @pl.when(middle)
        def _():
            drained("relay", full.at[pl.ds(0, 3), 0])
            drained("relay_w", weights.at[pl.ds(0, 4)])


def deliver(*refs):
    half = (len(refs) - 1) // 2
    copies = [pltpu.make_async_copy(src, dst, refs[-1].at[i])
              for i, (src, dst) in enumerate(zip(refs[:half], refs[half:-1]))]
    for copy in copies:
        copy.start()
    for copy in copies:
        copy.wait()


def dense(tokens, cotangent, routes, route_weight, w_gate, w_up, w_down):
    f32, bf16 = jnp.float32, jnp.bfloat16
    rows, width = tokens.shape
    ep, tp = lax.axis_size("ep"), lax.axis_size("tp")
    cols, half, nz, hidden = width // tp, rows // 2, ep // 2, w_gate.shape[2]
    anywhere, near = pl.BlockSpec(memory_space=pltpu.HBM), pl.BlockSpec(memory_space=pltpu.VMEM)

    def held(space, *arrays):
        return [pltpu.with_memory_space_constraint(x, space) for x in arrays]

    shapes = ((rows, cols), bf16), (routes.T.shape, f32), (w_gate.shape, f32), (w_up.shape, f32), (w_down.shape, f32)
    parts = pl.pallas_call(
        functools.partial(kernel, ep, tp),
        out_shape=tuple(pltpu.VMEM(*shape) for shape in shapes),
        in_specs=[anywhere, anywhere, near, near, anywhere, anywhere, anywhere],
        out_specs=(near,) * 5,
        scratch_shapes=[
            pltpu.VMEM((ep, 2, tp, rows, cols), bf16),
            pltpu.VMEM((width, hidden), bf16),
            pltpu.VMEM((width, hidden), bf16),
            pltpu.VMEM((hidden, width), bf16),
            pltpu.VMEM((ep, ep, rows), f32),
            pltpu.VMEM((ep, tp, rows, cols), bf16),
            pltpu.VMEM((nz, tp, rows, cols), bf16),
            pltpu.VMEM((nz, 4, half, cols), bf16),
            pltpu.VMEM((nz, 4, half, cols), bf16),
            pltpu.VMEM((nz, 2, half, cols), bf16),
            pltpu.VMEM((nz, 2, half, cols), bf16),
            pltpu.VMEM((nz, half, cols), bf16),
            pltpu.VMEM((nz, half, cols), bf16),
            pltpu.VMEM((nz - 1, rows, cols), bf16),
            pltpu.VMEM((nz, rows, cols), bf16),
            pltpu.VMEM((ep, rows, hidden), bf16),
            pltpu.VMEM((ep, rows, hidden), bf16),
            pltpu.VMEM((ep, rows, hidden), bf16),
            pltpu.VMEM((ep, 8, rows), f32),
            pltpu.VMEM((ep, rows), f32),
            pltpu.VMEM((tp, ep, rows), f32),
            pltpu.VMEM((ep, rows), f32),
            pltpu.VMEM((ep, ep, rows), f32),
            pltpu.SemaphoreType.DMA((4,)),
            pltpu.SemaphoreType.DMA((10,)),
            pltpu.SemaphoreType.DMA((19 * nz - 3,)),
        ],
        compiler_params=pltpu.CompilerParams(
            collective_id=0, has_side_effects=True, vmem_limit_bytes=50 * 1024 * 1024),
    )(*held(pltpu.HBM, tokens, cotangent), routes.T, route_weight.T,
      *held(pltpu.HBM, w_gate, w_up, w_down))
    grad_tokens, grw, *grads = pl.pallas_call(
        deliver,
        out_shape=tuple(jax.ShapeDtypeStruct(*shape) for shape in shapes),
        in_specs=[near] * 5,
        out_specs=(anywhere,) * 5,
        scratch_shapes=[pltpu.SemaphoreType.DMA((5,))],
        compiler_params=pltpu.CompilerParams(vmem_limit_bytes=1 << 20),
    )(*held(pltpu.VMEM, *parts))
    return grad_tokens, grw.T, *grads


def on_device(*args):
    rows, width = args[0].shape
    ep, tp = lax.axis_size("ep"), lax.axis_size("tp")
    fits = tp == 4 and ep == 8 and rows % 128 == 0 and 4 * rows * width * ep <= 1 << 24
    return (dense if fits else slotted)(*args)


def solution(mesh):
    return jax.shard_map(
        on_device,
        mesh=mesh,
        in_specs=(
            P("ep", None),
            P("ep", None),
            P("ep", None),
            P("ep", None),
            P("ep", None, "tp"),
            P("ep", None, "tp"),
            P("ep", "tp", None),
        ),
        out_specs=(
            P("ep", "tp"),
            P("ep", None),
            P("ep", None, "tp"),
            P("ep", None, "tp"),
            P("ep", "tp", None),
        ),
        check_vma=False,
    )
```

time: 80.3 us -> 68.9 us (0.86)
  the two profiles are of different devices: /device:TPU:0 before, /device:TPU:8 now
where the time goes in v2:
time: 68.9 us; the launch traced here: 68.7 us
  Pallas kernels  68.1 us (99%)
    pallas_call x1, Pallas kernels, dense(): pl.pallas_call(functools.partial(kernel, ep, tp), out_shape=tuple((pltpu....  65.3 us
    pallas_call x1, Pallas kernels, dense(): pl.pallas_call(deliver, out_shape=tuple((jax.ShapeDtypeStruct(*shape) for...  2.79 us

profile of v2, /device:TPU:8, one launch (start us, length us, event | category | flops | bytes accessed | tf_op | source)
XLA Modules:
  0.0 68.7 jit_solution(7240608434371593911)
XLA Ops:
  0.6 65.3 %shard_map.110 = (bf16[128,512]{1,0:T(8,128)(2,1)S(1)}, f32[2,128]{1,0:T(2,128)S(1)}, f32[1,2048,256]{2,1,0:T(8,128)S(1)}, f32[1,2048,256]{2,1,0:T(8,128)S(1)}, f32[1,256,2048]{2,1,0:T(8,128)S(1)}) custom-call(bf16[128,2048]{1,0:T(8,128)(2,1)} %tokens.1, bf16[128,2048]{1,0:T(8,128)(2,1)} %cotangent.1, s32[2,128]{1,0:T(2,128)} %bitcast.3, f32[2,128]{1,0:T(2,128)} %bitcast.4, ...), custom_call_target="tpu_custom_call" | custom-call | tf_op jit(solution)/shard_map/pallas_call | solution.py:489
  65.9 2.8 %shard_map.111 = (bf16[128,512]{1,0:T(8,128)(2,1)}, f32[2,128]{1,0:T(2,128)}, f32[1,2048,256]{2,1,0:T(8,128)}, f32[1,2048,256]{2,1,0:T(8,128)}, f32[1,256,2048]{2,1,0:T(8,128)}) custom-call(bf16[128,512]{1,0:T(8,128)(2,1)S(1)} %get-tuple-element.15.refs_0_, f32[2,128]{1,0:T(2,128)S(1)} %get-tuple-element.16.refs_1_, ...), custom_call_target="tpu_custom_call" | custom-call | tf_op jit(solution)/shard_map/pallas_call | solution.py:526

commit v3 on v2

--- a/solution.py
+++ b/solution.py
@@ -104,10 +104,22 @@
     return (grad_tokens, grad_route_weight, grad_gate, grad_up, grad_down)
 
 
+ORDER = (
+    ("fwd", 0), ("near", 0), ("near", 1), ("bwd", 0), ("near", 2), ("relayx", 1), ("relayy", 1), ("near", 3),
+    ("far", 0), ("far", 1), ("crossed", 1), ("diag", 1), ("far", 2), ("near", 4), ("far", 3), ("last", 0),
+    ("fwd", 1), ("last", 1), ("bwd", 1), ("relayx", 2), ("relayy", 2), ("last", 2), ("hand", 1),
+    ("relayx", 3), ("crossed", 2), ("relayy", 3), ("far", 4), ("diag", 2), ("last", 3), ("fwd", 2),
+    ("bwd", 2), ("diag", 3), ("first", 2), ("crossed", 3), ("last", 4), ("firstB", 2), ("fwd", 3),
+    ("second", 2), ("bwd", 3), ("tally",), ("first", 3), ("wg", 2), ("firstB", 3), ("third", 2), ("wg", 1),
+    ("homeward",), ("second", 3), ("first", 0), ("firstB", 0), ("third", 3), ("second", 0), ("wg", 3),
+    ("third", 0),
+)
+
+
 def kernel(ep, tp, tokens, cotangent, routes, route_weight, w_gate, w_up, w_down,
            result, out_home, g_gate, g_up, g_down,
            full, gate_v, up_v, down_v, weights, part, other, top, bottom,
-           in_top, in_bottom, last_top, last_bottom, share, arrived,
+           in_top, in_bottom, last_top, last_bottom, share, arrived, early,
            d_gate, d_up, act_w, score, score_rows, scores, total, home,
            local, sent, got):
     f32, bf16 = jnp.float32, jnp.bfloat16
@@ -124,12 +136,11 @@
     onward = jnp.where(z < nz // 2, 1, -1)
     middle = jnp.logical_and(z > 0, z < nz - 1)
     outer = jnp.logical_not(middle)
-    lead = jnp.where(middle, onward, 0)
-    back = [z, z + onward - 2 * lead, z + 2 * onward, z + 3 * onward - 2 * lead]
-    behind, ahead = z + onward - 2 * lead, z + onward
+    ahead, behind = z + onward, z - jnp.where(middle, onward, -onward)
+    back = [z, ahead, z + 2 * onward, z + jnp.where(middle, -1, 3) * onward]
+    groups = {name: i for i, name in enumerate(
+        ("pair", "plane", "side", "own", "hand", "quarters", "home", "small", "relay", "relay_w"))}
     names = {}
-    groups = {"pair": 0, "plane": 1, "side": 2, "own": 3, "halves": 4, "quarters": 5, "home": 6, "small": 7,
-              "relay": 8, "relay_w": 9}
 
     def scope(name):
         return jax.named_scope(name)
@@ -167,9 +178,10 @@
              for i, (src, dst) in enumerate(((w_gate, gate_v), (w_up, up_v), (w_down, down_v)))]
     for copy in own + loads:
         copy.start()
-    slot("along", 4 * nz), slot("x", 2 * nz - 2), slot("y", 2 * nz - 2), slot("dx", nz - 1), slot("dy", nz - 1)
-    slot("side", nz), slot("side_w", nz), slot("pair", 3 * nz), slot("top", nz), slot("bottom", nz)
-    slot("last_top", nz), slot("last_bottom", nz), slot("share"), slot("score"), slot("home")
+    for name, count in (("along", 6 * nz), ("x", 9), ("y", 9), ("dx", 3), ("dy", 3), ("side", 4), ("side_w", 4),
+                        ("pair", 4), ("pairs", 4), ("top", 4), ("tops", 4), ("bottom", 4), ("bottoms", 4),
+                        ("last_top", 4), ("last_bottom", 4), ("early", 1), ("share", 1), ("score", 1), ("home", 1)):
+        slot(name, count)
 
     barrier = pltpu.get_barrier_semaphore()
 
@@ -187,38 +199,46 @@
     hits = [named == routes[pl.ds(k, 1), :] for k in range(routes.shape[0])]
     weights[e] = sum(jnp.where(hit, route_weight[pl.ds(k, 1), :], 0.0) for k, hit in enumerate(hits))
 
+    @pl.when(outer)
+    def _():
+        early[...] = jnp.zeros_like(early)
+
     with scope("own"):
         pltpu.make_async_copy(full.at[e], full.at[e], local.at[0]).wait()
     with scope("barrier"):
         pl.semaphore_wait(barrier, jnp.where(middle, 5, 4))
 
     def pieces(s):
-        return full.at[s, 0, t], full.at[s, 1, t], full.at[s, 1, td], weights.at[s]
+        return (full.at[s, 0, t, :half], full.at[s, 0, t, half:], full.at[s, 1, t, :half], full.at[s, 1, t, half:],
+                full.at[s, 1, td], weights.at[s])
 
     def along(block, k):
-        return slot("along") + block * 4 + k
+        return slot("along") + block * 6 + k
 
     for k, piece in enumerate(pieces(e)):
-        push("small" if k == 3 else "own", piece, piece, along(z, k), ahead * 2 + c, t)
-        copy = plan("relay_w" if k == 3 else "relay", piece, piece, along(z, k), behind * 2 + c, t)
+        push("small" if k == 5 else "own", piece, piece, along(z, k), ahead * 2 + c, t)
+        copy = plan("relay_w" if k == 5 else "relay", piece, piece, along(z, k), behind * 2 + c, t)
         pl.when(middle)(copy.start)
     push("small", weights.at[e], weights.at[e], slot("side_w"), side, t)
     push("side", full.at[e], full.at[e], slot("side"), side, t)
 
     def step(dz, k, onto, only=None):
         block = back[dz]
-        piece = pieces(block * 2 + c)[k]
+        s = block * 2 + c
+        piece = pieces(s)[k]
         arrival = landing(piece, along(block, k))
+        copies = []
         if only is not outer:
-            passed = plan("relay_w" if k == 3 else "relay", piece, piece, along(block, k), onto * 2 + c, t)
-        copies = []
-        if k < 2:
-            copies.append(plan("plane", piece, piece, slot("x") + dz * 2 - 2 + k, e, tx))
-            copies.append(plan("plane", piece, piece, slot("y") + dz * 2 - 2 + k, e, ty))
-        if k == 3:
+            passed = plan("relay_w" if k == 5 else "relay", piece, piece, along(block, k), onto * 2 + c, t)
+        if k < 4:
+            to = dz * 3 - 3 + min(k, 2)
+            copies.append(plan("plane", piece, piece, slot("x") + to, e, tx))
+            copies.append(plan("plane", piece, piece, slot("y") + to, e, ty))
+        if k == 5:
             copies.append(plan("small", piece, piece, slot("side_w") + dz, side, t))
-        else:
-            copies.append(plan("side", piece, piece, slot("side") + dz, side, t))
+        elif k % 2 or k == 4:
+            whole = {1: full.at[s, 0, t], 3: full.at[s, 1, t], 4: piece}[k]
+            copies.append(plan("side", whole, whole, slot("side") + dz, side, t))
 
         def run():
             arrival.wait_recv()
@@ -233,38 +253,45 @@
             run() if only is None else pl.when(only)(run)
 
     def near(k):
-        step(1, k, ahead)
-        step(3, k, behind, middle)
+        for k in (4, 5) if k == 4 else (k,):
+            step(1, k, behind)
+            step(3, k, ahead, middle)
 
     def far(k):
-        step(2, k, behind)
+        for k in (4, 5) if k == 4 else (k,):
+            step(2, k, behind)
 
     def last(k):
-        step(3, k, behind, outer)
+        for k in (4, 5) if k == 4 else (k,):
+            step(3, k, behind, outer)
 
     def aside(dz, a, q):
         piece = full.at[back[dz] * 2 + c, a, q]
         push("side", piece, piece, slot("side") + dz, side, t)
 
-    def relay(dz):
+    def relayx(dz):
+        piece = full.at[back[dz] * 2 + c, 0, ty, :half]
+        landed(piece, slot("y") + dz * 3 - 3, f"y0_{dz}")
+        push("quarters", piece, piece, slot("dx") + dz - 1, e, tx)
+
+    def relayy(dz):
         s = back[dz] * 2 + c
-        landed(full.at[s, 0, ty], slot("y") + dz * 2 - 2, f"y0_{dz}")
-        piece = full.at[s, 0, ty, :half]
-        push("quarters", piece, piece, slot("dx") + dz - 1, e, tx)
-        landed(full.at[s, 0, tx], slot("x") + dz * 2 - 2, f"x0_{dz}")
         piece = full.at[s, 0, tx, half:]
+        landed(piece, slot("x") + dz * 3 - 2, f"x1_{dz}")
         push("quarters", piece, piece, slot("dy") + dz - 1, e, ty)
+        landed(full.at[s, 0, ty, half:], slot("y") + dz * 3 - 2, f"y1_{dz}")
         aside(dz, 0, ty)
+        landed(full.at[s, 0, tx, :half], slot("x") + dz * 3 - 3, f"x0_{dz}")
         aside(dz, 0, tx)
 
     def crossed(dz):
         s = back[dz] * 2 + c
-        landed(full.at[s, 1, ty], slot("y") + dz * 2 - 1, f"y1_{dz}")
+        landed(full.at[s, 1, ty], slot("y") + dz * 3 - 1, f"y2_{dz}")
         aside(dz, 1, ty)
-        landed(full.at[s, 1, tx], slot("x") + dz * 2 - 1, f"x1_{dz}")
+        landed(full.at[s, 1, tx], slot("x") + dz * 3 - 1, f"x2_{dz}")
         aside(dz, 1, tx)
 
-    def diagonal(dz):
+    def diag(dz):
         s = back[dz] * 2 + c
         landed(full.at[s, 0, td, :half], slot("dx") + dz - 1, f"dx_{dz}")
         landed(full.at[s, 0, td, half:], slot("dy") + dz - 1, f"dy_{dz}")
@@ -281,7 +308,7 @@
         row = jnp.sum(jnp.where(mine, weights[block], 0.0), axis=0, keepdims=True)
         return jnp.transpose(jnp.broadcast_to(row, (rows, rows)))[:, :1]
 
-    def forward(dz):
+    def fwd(dz):
         b = back[dz] * 2
         landed(full.at[b + 1 - c], slot("side") + dz, f"side_{dz}")
         landed(weights.at[b + 1 - c], slot("side_w") + dz, f"sidew_{dz}")
@@ -311,7 +338,7 @@
                 act_w[b + i] = aw[cut]
                 score[b + i] = jnp.transpose(jnp.broadcast_to(sums[cut], (rows, rows)))[:8]
 
-    def backward(dz):
+    def bwd(dz):
         b = back[dz] * 2
         with scope(f"bwd_{dz}"):
             dg = jnp.concatenate([d_gate[b], d_gate[b + 1]], axis=0)
@@ -321,7 +348,7 @@
                 piece = (nt(dg, gate_v[span, :]) + nt(du, up_v[span, :])).astype(bf16)
                 part[b, q] = piece[:rows]
                 part[b + 1, q] = piece[rows:]
-                push("pair", part.at[b + 1 - c, q], other.at[dz, q], slot("pair") + dz * 3 + max(r - 1, 0), side, t)
+                push("pair", part.at[b + 1 - c, q], other.at[dz, q], slot("pairs" if r else "pair") + dz, side, t)
 
     def add(*terms):
         value = terms[0].astype(f32)
@@ -329,47 +356,62 @@
             value = value + term.astype(f32)
         return value
 
+    def paired(dz, q, cut=slice(None)):
+        terms = [part[back[dz] * 2 + c, q, cut], other[dz, q, cut]]
+        return add(*terms, *([early[0, q, cut], early[1, q, cut]] if dz == 0 else [])).astype(bf16)
+
+    upper, lower = slice(0, half), slice(half, rows)
+
+    def hand(dz):
+        landed(other.at[dz, td], slot("pair") + dz, f"pair_{dz}")
+        landed(other.at[dz, pl.ds(0, 3)], slot("pairs") + dz, f"pairs_{dz}")
+        s = back[dz] * 2 + c
+        for q in range(tp):
+            part[s, q] = paired(dz, q)
+            push("hand", part.at[s, q], early.at[jnp.where(middle, 1, 0), q], slot("early"), ahead * 2 + c, t)
+
     def first(dz):
-        s = back[dz] * 2 + c
-
-        def both(q, upper):
-            cut = slice(0, half) if upper else slice(half, rows)
-            return add(part[s, q, cut], other[dz, q, cut]).astype(bf16)
-
-        landed(other.at[dz, pl.ds(0, 2)], slot("pair") + dz * 3, f"pair0_{dz}")
-        top[dz, 3] = both(td, True)
-        top[dz, 2] = both(tx, True)
-        push("halves", top.at[dz, pl.ds(2, 2)], in_top.at[dz], slot("top") + dz, e, tx)
-        landed(other.at[dz, ty], slot("pair") + dz * 3 + 1, f"pair2_{dz}")
-        bottom[dz, 3] = both(td, False)
-        bottom[dz, 2] = both(ty, False)
-        push("halves", bottom.at[dz, pl.ds(2, 2)], in_bottom.at[dz], slot("bottom") + dz, e, ty)
-        landed(other.at[dz, t], slot("pair") + dz * 3 + 2, f"pair3_{dz}")
-        top[dz, 0] = both(t, True)
-        top[dz, 1] = both(ty, True)
-        bottom[dz, 0] = both(t, False)
-        bottom[dz, 1] = both(tx, False)
+        landed(other.at[dz, td], slot("pair") + dz, f"pair_{dz}")
+        if dz == 0:
+            with scope("early"):
+                pl.when(middle)(landing(early, slot("early")).wait_recv)
+        top[dz, 3] = paired(dz, td, upper)
+        push("quarters", top.at[dz, 3], in_top.at[dz, 1], slot("top") + dz, e, tx)
+        bottom[dz, 3] = paired(dz, td, lower)
+        push("quarters", bottom.at[dz, 3], in_bottom.at[dz, 1], slot("bottom") + dz, e, ty)
+
+    def firstB(dz):
+        landed(other.at[dz, pl.ds(0, 3)], slot("pairs") + dz, f"pairs_{dz}")
+        top[dz, 2] = paired(dz, tx, upper)
+        push("quarters", top.at[dz, 2], in_top.at[dz, 0], slot("tops") + dz, e, tx)
+        bottom[dz, 2] = paired(dz, ty, lower)
+        push("quarters", bottom.at[dz, 2], in_bottom.at[dz, 0], slot("bottoms") + dz, e, ty)
+        top[dz, 1] = paired(dz, ty, upper)
+        bottom[dz, 1] = paired(dz, tx, lower)
+        top[dz, 0] = paired(dz, t, upper)
+        bottom[dz, 0] = paired(dz, t, lower)
 
     def second(dz):
-        landed(in_top.at[dz], slot("top") + dz, f"top_{dz}")
+        landed(in_top.at[dz, 1], slot("top") + dz, f"top_{dz}")
         top[dz, 1] = add(top[dz, 1], in_top[dz, 1]).astype(bf16)
         push("quarters", top.at[dz, 1], last_top.at[dz], slot("last_top") + dz, e, ty)
-        landed(in_bottom.at[dz], slot("bottom") + dz, f"bottom_{dz}")
+        landed(in_bottom.at[dz, 1], slot("bottom") + dz, f"bottom_{dz}")
         bottom[dz, 1] = add(bottom[dz, 1], in_bottom[dz, 1]).astype(bf16)
         push("quarters", bottom.at[dz, 1], last_bottom.at[dz], slot("last_bottom") + dz, e, tx)
 
+    kept = []
+
     def third(dz):
-        halves = []
         for cut, mine, got_in, ending, name in (
-                (pl.ds(0, half), top, in_top, last_top, "last_top"),
-                (pl.ds(half, half), bottom, in_bottom, last_bottom, "last_bottom")):
-            landed(ending.at[dz], slot(name) + dz, f"{name}_{dz}")
+                (pl.ds(0, half), top, in_top, last_top, "top"), (pl.ds(half, half), bottom, in_bottom, last_bottom, "bottom")):
+            landed(got_in.at[dz, 0], slot(name + "s") + dz, f"{name}s_{dz}")
+            landed(ending.at[dz], slot("last_" + name) + dz, f"last_{name}_{dz}")
             value = add(mine[dz, 0], got_in[dz, 0], ending[dz])
             if dz:
-                share[dz - 1, cut] = value.astype(bf16)
-                push("quarters", share.at[dz - 1, cut], arrived.at[z, cut], slot("share"), back[dz] * 2 + c, t)
-            halves.append(value)
-        return halves
+                share[dz - 2, cut] = value.astype(bf16)
+                push("quarters", share.at[dz - 2, cut], arrived.at[z, cut], slot("share"), back[dz] * 2 + c, t)
+            else:
+                kept.append(value)
 
     def by_width(out, ref, name):
         with scope(name):
@@ -380,69 +422,46 @@
     with scope("loads"):
         for copy in loads:
             copy.wait()
-    forward(0)
-    near(0)
-    backward(0)
-    near(1)
-    first(0)
-    relay(1)
-    near(2)
-    near(3)
-    crossed(1)
-    far(0)
-    diagonal(1)
-    second(0)
-    forward(1)
-    far(1)
-    backward(1)
-    relay(2)
-    first(1)
-    far(2)
-    far(3)
-    crossed(2)
-    last(0)
-    diagonal(2)
-    forward(2)
-    last(1)
-    backward(2)
-    second(1)
-    relay(3)
-    last(2)
-    last(3)
-    first(2)
-    crossed(3)
-    third(1)
-    diagonal(3)
-    forward(3)
-    backward(3)
-    second(2)
-    score_rows[...] = jnp.concatenate([score[j, :1] for j in range(ep)], axis=0)
-    for k in range(1, tp):
-        push("small", score_rows, scores.at[t], slot("score"), e, lax.rem(t + k, tp))
-    scores[t] = score_rows[...]
-    third(2)
-    first(3)
-    by_width(g_gate, d_gate, "wg_gate")
-    landed(scores.at[pl.ds(0, tp - 1)], slot("score"), "score")
-    total[...] = add(*[scores[j] for j in range(tp)])
-    for k in range(1, ep):
-        push("home", total, home.at[e], slot("home"), lax.rem(e + k, ep), t)
-    home[e] = total[...]
-    by_width(g_up, d_up, "wg_up")
-    second(3)
-    with scope("wg_down"):
-        left = act_w[...].reshape(ep * rows, act_w.shape[2])
-        for q in range(tp):
-            g_down[0, :, pl.ds(q * cols, cols)] = tn(left, full[:, 1, q].reshape(ep * rows, cols))
-    third(3)
-    upper, lower = third(0)
-    landed(arrived.at[pl.ds(0, nz - 1)], slot("share"), "arrived")
-    for k in range(1, nz):
-        j = lax.rem(z + k, nz)
-        upper = upper + arrived[j, :half].astype(f32)
-        lower = lower + arrived[j, half:].astype(f32)
-    result[:half] = upper.astype(bf16)
-    result[half:] = lower.astype(bf16)
+    def wg(i):
+        if i == 1:
+            by_width(g_gate, d_gate, "wg_gate")
+        elif i == 2:
+            by_width(g_up, d_up, "wg_up")
+        else:
+            with scope("wg_down"):
+                left = act_w[...].reshape(ep * rows, act_w.shape[2])
+                for q in range(tp):
+                    g_down[0, :, pl.ds(q * cols, cols)] = tn(left, full[:, 1, q].reshape(ep * rows, cols))
+
+    def tally():
+        score_rows[...] = jnp.concatenate([score[j, :1] for j in range(ep)], axis=0)
+        for k in range(1, tp):
+            push("small", score_rows, scores.at[t], slot("score"), e, lax.rem(t + k, tp))
+        scores[t] = score_rows[...]
+
+    def homeward():
+        landed(scores.at[pl.ds(0, tp - 1)], slot("score"), "score")
+        total[...] = add(*[scores[j] for j in range(tp)])
+        for k in range(1, ep):
+            push("home", total, home.at[e], slot("home"), lax.rem(e + k, ep), t)
+        home[e] = total[...]
+
+    steps = locals()
+    for name, *where in ORDER:
+        steps[name](*where)
+
+    @pl.when(middle)
+    def _():
+        landed(arrived.at[pl.ds(0, 1)], slot("share"), "arrived_m")
+        for cut, value in zip((upper, lower), kept):
+            result[cut] = add(value, arrived[back[2], cut]).astype(bf16)
+
+    @pl.when(outer)
+    def _():
+        landed(arrived.at[pl.ds(0, nz - 1)], slot("share"), "arrived_o")
+        for cut, value in zip((upper, lower), kept):
+            result[cut] = add(value, *[arrived[back[i], cut] for i in (1, 2, 3)]).astype(bf16)
+
     landed(home.at[pl.ds(0, ep - 1)], slot("home"), "home")
     back_home = jnp.concatenate(
         [jnp.sum(jnp.where(named == e, home[j], 0.0), axis=0, keepdims=True) for j in range(ep)], axis=0)
@@ -454,8 +473,8 @@
         drained("plane", full.at[pl.ds(0, 3), 0])
         drained("side", full.at[pl.ds(0, 4)])
         drained("own", full.at[0, 0, pl.ds(0, 3)])
-        drained("halves", full.at[0])
-        drained("quarters", full.at[pl.ds(0, 5), 0, pl.ds(0, 2)])
+        drained("hand", full.at[0, 0])
+        drained("quarters", full.at[pl.ds(0, 7), 0, pl.ds(0, 2)])
         drained("home", weights.at[pl.ds(0, ep - 1)])
         drained("small", weights)
 
@@ -505,8 +524,9 @@
             pltpu.VMEM((nz, 2, half, cols), bf16),
             pltpu.VMEM((nz, half, cols), bf16),
             pltpu.VMEM((nz, half, cols), bf16),
-            pltpu.VMEM((nz - 1, rows, cols), bf16),
+            pltpu.VMEM((2, rows, cols), bf16),
             pltpu.VMEM((nz, rows, cols), bf16),
+            pltpu.VMEM((2, tp, rows, cols), bf16),
             pltpu.VMEM((ep, rows, hidden), bf16),
             pltpu.VMEM((ep, rows, hidden), bf16),
             pltpu.VMEM((ep, rows, hidden), bf16),
@@ -517,7 +537,7 @@
             pltpu.VMEM((ep, ep, rows), f32),
             pltpu.SemaphoreType.DMA((4,)),
             pltpu.SemaphoreType.DMA((10,)),
-            pltpu.SemaphoreType.DMA((19 * nz - 3,)),
+            pltpu.SemaphoreType.DMA((92,)),
         ],
         compiler_params=pltpu.CompilerParams(
             collective_id=0, has_side_effects=True, vmem_limit_bytes=50 * 1024 * 1024),

time: 68.9 us -> 60.7 us (0.88)
  the two profiles are of different devices: /device:TPU:8 before, /device:TPU:0 now
where the time goes in v3:
time: 60.7 us; the launch traced here: 60.5 us
  Pallas kernels  59.9 us (99%)
  between operations  0.64 us (1%)
    pallas_call x1, Pallas kernels, dense(): pl.pallas_call(functools.partial(kernel, ep, tp), out_shape=tuple((pltpu....  57.1 us
    pallas_call x1, Pallas kernels, dense(): pl.pallas_call(deliver, out_shape=tuple((jax.ShapeDtypeStruct(*shape) for...  2.79 us

profile of v3, /device:TPU:0, one launch (start us, length us, event | category | flops | bytes accessed | tf_op | source)
XLA Modules:
  0.0 60.5 jit_solution(3342961705586448052)
XLA Ops:
  0.6 57.1 %shard_map.110 = (bf16[128,512]{1,0:T(8,128)(2,1)S(1)}, f32[2,128]{1,0:T(2,128)S(1)}, f32[1,2048,256]{2,1,0:T(8,128)S(1)}, f32[1,2048,256]{2,1,0:T(8,128)S(1)}, f32[1,256,2048]{2,1,0:T(8,128)S(1)}) custom-call(bf16[128,2048]{1,0:T(8,128)(2,1)} %tokens.1, bf16[128,2048]{1,0:T(8,128)(2,1)} %cotangent.1, s32[2,128]{1,0:T(2,128)} %bitcast.3, f32[2,128]{1,0:T(2,128)} %bitcast.4, ...), custom_call_target="tpu_custom_call" | custom-call | tf_op jit(solution)/shard_map/pallas_call | solution.py:508
  57.7 2.8 %shard_map.111 = (bf16[128,512]{1,0:T(8,128)(2,1)}, f32[2,128]{1,0:T(2,128)}, f32[1,2048,256]{2,1,0:T(8,128)}, f32[1,2048,256]{2,1,0:T(8,128)}, f32[1,256,2048]{2,1,0:T(8,128)}) custom-call(bf16[128,512]{1,0:T(8,128)(2,1)S(1)} %get-tuple-element.15.refs_0_, f32[2,128]{1,0:T(2,128)S(1)} %get-tuple-element.16.refs_1_, ...), custom_call_target="tpu_custom_call" | custom-call | tf_op jit(solution)/shard_map/pallas_call | solution.py:546

commit v4 on v3

v4 whole, which is shorter than its diff:
```python
import functools

import jax
import jax.numpy as jnp
from jax import lax
from jax.experimental import pallas as pl
from jax.experimental.pallas import tpu as pltpu
from jax.sharding import PartitionSpec as P


def slot_index(block_routes, experts, capacity):
    flat_ids = block_routes.reshape(-1)
    onehot = (flat_ids[:, None] == jnp.arange(experts, dtype=jnp.int32)[None, :]).astype(jnp.int32)
    earlier = jnp.cumsum(onehot, axis=0) - onehot
    return flat_ids * capacity + jnp.sum(earlier * onehot, axis=1)


def slotted(tokens, cotangent, routes, route_weight, w_gate, w_up, w_down):
    f32 = jnp.float32
    tok_rows, model_width = tokens.shape
    choices_row = routes.shape[1]
    experts = lax.axis_size("ep")
    capacity = 2 * tok_rows * choices_row // experts
    recv_rows = experts * capacity
    slot_ids = slot_index(routes, experts, capacity)
    send_w = jnp.zeros((recv_rows,), f32).at[slot_ids].set(route_weight.reshape(-1))
    send_x = (
        jnp.zeros((recv_rows, model_width), jnp.bfloat16)
        .at[slot_ids]
        .set(jnp.repeat(tokens, choices_row, axis=0))
    )
    send_dy = (
        jnp.zeros((recv_rows, model_width), jnp.bfloat16)
        .at[slot_ids]
        .set(jnp.repeat(cotangent, choices_row, axis=0))
    )
    got_x = lax.all_to_all(
        send_x.reshape(experts, capacity, model_width),
        "ep",
        split_axis=0,
        concat_axis=0,
        tiled=True,
    )
    got_dy, got_w = (
        lax.all_to_all(
            send_dy.reshape(experts, capacity, model_width),
            "ep",
            split_axis=0,
            concat_axis=0,
            tiled=True,
        ),
        lax.all_to_all(
            send_w.reshape(experts, capacity, 1).astype(jnp.bfloat16),
            "ep",
            split_axis=0,
            concat_axis=0,
            tiled=True,
        ).astype(jnp.float32),
    )
    rows_x = got_x.reshape(recv_rows, model_width)
    rows_dy = got_dy.reshape(recv_rows, model_width)
    rows_w = got_w.reshape(recv_rows)
    gate_w = w_gate[0]
    up_w = w_up[0]
    down_w = w_down[0]
    gate_pre = jnp.dot(rows_x, gate_w, preferred_element_type=f32)
    up_pre = jnp.dot(rows_x, up_w, preferred_element_type=f32)
    gate_sig = jax.nn.sigmoid(gate_pre)
    act_full = gate_pre * gate_sig * up_pre
    act = act_full.astype(jnp.bfloat16)
    back_hidden = jnp.einsum("rd,fd->rf", rows_dy, down_w, preferred_element_type=f32)
    weighted_cot = (rows_w[:, None] * rows_dy.astype(f32)).astype(jnp.bfloat16)
    d_hidden = rows_w[:, None] * back_hidden
    d_gate = (d_hidden * up_pre * gate_sig * (1.0 + gate_pre * (1.0 - gate_sig))).astype(
        jnp.bfloat16
    )
    d_up = (d_hidden * gate_pre * gate_sig).astype(jnp.bfloat16)
    gate_part = jnp.sum(act_full * back_hidden, axis=1)
    token_part = jnp.einsum("rf,df->rd", d_gate, gate_w, preferred_element_type=f32)
    token_part = token_part + jnp.einsum("rf,df->rd", d_up, up_w, preferred_element_type=f32)
    grad_gate = jnp.einsum("rd,rf->df", rows_x, d_gate, preferred_element_type=f32)[None]
    grad_up = jnp.einsum("rd,rf->df", rows_x, d_up, preferred_element_type=f32)[None]
    grad_down = jnp.einsum("rf,rd->fd", act, weighted_cot, preferred_element_type=f32)[None]
    rounded_part = token_part.astype(jnp.bfloat16).astype(f32)
    shares = lax.psum_scatter(
        rounded_part.astype(jnp.bfloat16), "tp", scatter_dimension=1, tiled=True
    )
    gate_total = lax.psum(gate_part, "tp")
    back_x, back_gate = (
        lax.all_to_all(
            shares.reshape(experts, capacity, -1), "ep", split_axis=0, concat_axis=0, tiled=True
        ),
        lax.all_to_all(
            gate_total.reshape(experts, capacity).astype(jnp.bfloat16),
            "ep",
            split_axis=0,
            concat_axis=0,
            tiled=True,
        ).astype(jnp.float32),
    )
    picked = back_x.reshape(recv_rows, -1)[slot_ids].astype(f32).reshape(tok_rows, choices_row, -1)
    grad_route_weight = back_gate.reshape(recv_rows)[slot_ids].reshape(tok_rows, choices_row)
    grad_tokens = jnp.sum(picked, axis=1).astype(jnp.bfloat16)
    return (grad_tokens, grad_route_weight, grad_gate, grad_up, grad_down)


def kernel(ep, tp, tokens, cotangent, routes, route_weight, w_gate, w_up, w_down,
           result, out_home, g_gate, g_up, g_down,
           full, in_v, down_v, weights, part, other, top, bottom,
           in_top, in_bottom, last_top, last_bottom, share, arrived, early,
           d_in, act_w, score, score_rows, scores, total, home,
           local, sent, got):
    f32, bf16 = jnp.float32, jnp.bfloat16
    rows, width = tokens.shape
    cols = width // tp
    half = rows // 2
    nz = ep // 2
    e, t = lax.axis_index("ep"), lax.axis_index("tp")
    z, c = e // 2, lax.rem(e, 2)
    y, x = t // 2, lax.rem(t, 2)
    side = z * 2 + 1 - c
    tx, ty = y * 2 + 1 - x, (1 - y) * 2 + x
    td = (1 - y) * 2 + 1 - x
    onward = jnp.where(z < nz // 2, 1, -1)
    middle = jnp.logical_and(z > 0, z < nz - 1)
    outer = jnp.logical_not(middle)
    ahead, behind = z + onward, z - jnp.where(middle, onward, -onward)
    back = [z, ahead, z + 2 * onward, z + jnp.where(middle, -1, 3) * onward]
    groups = {name: i for i, name in enumerate(
        ("pair", "plane", "side", "own", "hand", "quarters", "home", "small", "relay", "relay_w"))}
    names = {}

    def slot(name, count=1):
        if name not in names:
            names[name] = sum(n for _, n in names.values()), count
        return names[name][0]

    def plan(group, src, dst, slot_at, to_e, to_t):
        return pltpu.make_async_remote_copy(
            src_ref=src, dst_ref=dst, send_sem=sent.at[groups[group]], recv_sem=got.at[slot_at],
            device_id={"ep": to_e, "tp": to_t}, device_id_type=pl.DeviceIdType.MESH)

    def push(*args):
        plan(*args).start()

    def drained(group, ref):
        pltpu.make_async_remote_copy(
            src_ref=ref, dst_ref=ref, send_sem=sent.at[groups[group]], recv_sem=got.at[0],
            device_id={"ep": side, "tp": t}, device_id_type=pl.DeviceIdType.MESH).wait_send()

    def landing(dst, slot_at):
        return pltpu.make_async_remote_copy(
            src_ref=dst, dst_ref=dst, send_sem=sent.at[0], recv_sem=got.at[slot_at],
            device_id={"ep": side, "tp": t}, device_id_type=pl.DeviceIdType.MESH)

    def landed(dst, slot_at):
        landing(dst, slot_at).wait_recv()

    barrier = pltpu.get_barrier_semaphore()

    def greet(to_e, to_t):
        pl.semaphore_signal(barrier, inc=1, device_id={"ep": to_e, "tp": to_t},
                            device_id_type=pl.DeviceIdType.MESH)

    own_tiles = [pltpu.make_async_copy(ref.at[:, pl.ds(q * cols, cols)], full.at[e, a, q], local.at[0])
                 for a, ref in enumerate((tokens, cotangent)) for q in range(tp)]
    for copy in own_tiles:
        copy.start()
    greet(ahead * 2 + c, t)
    pl.when(middle)(lambda: greet(behind * 2 + c, t))
    greet(e, tx)
    greet(e, ty)
    greet(side, t)

    for name, count in (("along", 6 * nz), ("x", 9), ("y", 9), ("dx", 3), ("dy", 3), ("side", 4), ("side_w", 4),
                        ("pair", 4), ("pairs", 4), ("top", 3), ("tops", 3), ("bottom", 3), ("bottoms", 3),
                        ("last_top", 3), ("last_bottom", 3), ("early", 1), ("share", 1), ("score", 1), ("home", 1)):
        slot(name, count)

    def summed(name, dz):
        return slot(name) + max(dz - 1, 0)

    named = lax.broadcasted_iota(jnp.int32, (ep, rows), 0)
    hits = [named == routes[pl.ds(k, 1), :] for k in range(routes.shape[0])]
    weights[e] = sum(jnp.where(hit, route_weight[pl.ds(k, 1), :], 0.0) for k, hit in enumerate(hits))
    pltpu.make_async_copy(full.at[e], full.at[e], local.at[0]).wait()
    pl.semaphore_wait(barrier, jnp.where(middle, 5, 4))

    def pieces(s):
        return (full.at[s, 0, t, :half], full.at[s, 0, t, half:], full.at[s, 1, t, :half], full.at[s, 1, t, half:],
                full.at[s, 1, td], weights.at[s])

    def along(block, k):
        return slot("along") + block * 6 + k

    for k, piece in enumerate(pieces(e)):
        push("small" if k == 5 else "own", piece, piece, along(z, k), ahead * 2 + c, t)
        copy = plan("relay_w" if k == 5 else "relay", piece, piece, along(z, k), behind * 2 + c, t)
        pl.when(middle)(copy.start)
    hidden = down_v.shape[0]
    loads = [pltpu.make_async_copy(src.at[0], dst, local.at[1 + i]) for i, (src, dst) in enumerate((
        (w_gate, in_v.at[:, pl.ds(0, hidden)]), (w_up, in_v.at[:, pl.ds(hidden, hidden)]), (w_down, down_v)))]
    for copy in loads:
        copy.start()

    @pl.when(outer)
    def _():
        early[...] = jnp.zeros_like(early)

    def own():
        push("small", weights.at[e], weights.at[e], slot("side_w"), side, t)
        push("side", full.at[e], full.at[e], slot("side"), side, t)
        for copy in loads:
            copy.wait()

    onto = {}

    def step(dz, k):
        if k == 6:
            return
        block = back[dz]
        s = block * 2 + c
        piece = pieces(s)[k]
        landed(piece, along(block, k))
        if dz in onto:
            push("relay_w" if k == 5 else "relay", piece, piece, along(block, k), onto[dz] * 2 + c, t)
        if k < 4:
            to = dz * 3 - 3 + min(k, 2)
            push("plane", piece, piece, slot("x") + to, e, tx)
            push("plane", piece, piece, slot("y") + to, e, ty)
        if k == 5:
            push("small", piece, piece, slot("side_w") + dz, side, t)
        elif k % 2 or k == 4:
            whole = {1: full.at[s, 0, t], 3: full.at[s, 1, t], 4: piece}[k]
            push("side", whole, whole, slot("side") + dz, side, t)
        if k == 4:
            step(dz, 5)

    def near(k):
        step(1, k)

    def far(k):
        step(2, k)

    def last(k):
        step(3, k)

    def aside(dz, a, q):
        piece = full.at[back[dz] * 2 + c, a, q]
        push("side", piece, piece, slot("side") + dz, side, t)

    def relayx(dz):
        piece = full.at[back[dz] * 2 + c, 0, ty, :half]
        landed(piece, slot("y") + dz * 3 - 3)
        push("quarters", piece, piece, slot("dx") + dz - 1, e, tx)

    def relayy(dz):
        s = back[dz] * 2 + c
        piece = full.at[s, 0, tx, half:]
        landed(piece, slot("x") + dz * 3 - 2)
        push("quarters", piece, piece, slot("dy") + dz - 1, e, ty)
        landed(full.at[s, 0, ty, half:], slot("y") + dz * 3 - 2)
        aside(dz, 0, ty)
        landed(full.at[s, 0, tx, :half], slot("x") + dz * 3 - 3)
        aside(dz, 0, tx)

    def crossed(dz):
        s = back[dz] * 2 + c
        landed(full.at[s, 1, ty], slot("y") + dz * 3 - 1)
        aside(dz, 1, ty)
        landed(full.at[s, 1, tx], slot("x") + dz * 3 - 1)
        aside(dz, 1, tx)

    def diag(dz):
        s = back[dz] * 2 + c
        landed(full.at[s, 0, td, :half], slot("dx") + dz - 1)
        landed(full.at[s, 0, td, half:], slot("dy") + dz - 1)
        aside(dz, 0, td)

    def nt(a, b):
        return lax.dot_general(a, b, (((1,), (1,)), ((), ())), preferred_element_type=f32)

    def tn(a, b):
        return lax.dot_general(a, b, (((0,), (0,)), ((), ())), preferred_element_type=f32)

    def column(block):
        mine = lax.broadcasted_iota(jnp.int32, (ep, rows), 0) == e
        row = jnp.sum(jnp.where(mine, weights[block], 0.0), axis=0, keepdims=True)
        return jnp.transpose(jnp.broadcast_to(row, (rows, rows)))[:, :1]

    def fwd(dz):
        b = back[dz] * 2
        landed(full.at[b + 1 - c], slot("side") + dz)
        landed(weights.at[b + 1 - c], slot("side_w") + dz)
        gu = bk = None
        for q in range(tp):
            span = pl.ds(q * cols, cols)
            xs = jnp.concatenate([full[b, 0, q], full[b + 1, 0, q]], axis=0)
            dy = jnp.concatenate([full[b, 1, q], full[b + 1, 1, q]], axis=0)
            gu_q = jnp.dot(xs, in_v[span, :], preferred_element_type=f32)
            b_q = nt(dy, down_v[:, span])
            gu, bk = (gu_q, b_q) if q == 0 else (gu + gu_q, bk + b_q)
        g, u = gu[:, :hidden], gu[:, hidden:]
        w = jnp.concatenate([column(b), column(b + 1)], axis=0)
        sig = jax.nn.sigmoid(g)
        silu = g * sig
        act = silu * u
        d_h = w * bk
        dg = (d_h * u * sig * (1.0 + g * (1.0 - sig))).astype(bf16)
        du = (d_h * silu).astype(bf16)
        aw = (w * act).astype(bf16)
        sums = jnp.sum(act * bk, axis=1, keepdims=True)
        for i in range(2):
            cut = slice(i * rows, (i + 1) * rows)
            d_in[b + i, :, :hidden] = dg[cut]
            d_in[b + i, :, hidden:] = du[cut]
            act_w[b + i] = aw[cut]
            score[b + i] = jnp.transpose(jnp.broadcast_to(sums[cut], (rows, rows)))[:8]

    def bwd(dz):
        b = back[dz] * 2
        d = jnp.concatenate([d_in[b], d_in[b + 1]], axis=0)
        for group, name in (((td,), "pair"), ((tx, ty, t), "pairs")):
            for q in group:
                piece = nt(d, in_v[pl.ds(pl.multiple_of(q * cols, cols), cols), :]).astype(bf16)
                part[b, q] = piece[:rows]
                part[b + 1, q] = piece[rows:]
            for q in group:
                push("pair", part.at[b + 1 - c, q], other.at[dz, q], slot(name) + dz, side, t)

    def add(*terms):
        value = terms[0].astype(f32)
        for term in terms[1:]:
            value = value + term.astype(f32)
        return value

    def paired(dz, q, cut=slice(None)):
        terms = [part[back[dz] * 2 + c, q, cut], other[dz, q, cut]]
        return add(*terms, *([early[0, q, cut], early[1, q, cut]] if dz == 0 else [])).astype(bf16)

    upper, lower = slice(0, half), slice(half, rows)

    def hand(dz):
        landed(other.at[dz, td], slot("pair") + dz)
        landed(other.at[dz, pl.ds(0, 3)], slot("pairs") + dz)
        s = back[dz] * 2 + c
        for q in range(tp):
            part[s, q] = paired(dz, q)
            push("hand", part.at[s, q], early.at[jnp.where(middle, 1, 0), q], slot("early"), ahead * 2 + c, t)

    def first(dz):
        landed(other.at[dz, td], slot("pair") + dz)
        if dz == 0:
            if onto:
                landed(early, slot("early"))
        top[dz, 3] = paired(dz, td, upper)
        push("quarters", top.at[dz, 3], in_top.at[dz, 1], summed("top", dz), e, tx)
        bottom[dz, 3] = paired(dz, td, lower)
        push("quarters", bottom.at[dz, 3], in_bottom.at[dz, 1], summed("bottom", dz), e, ty)

    def firstB(dz):
        landed(other.at[dz, pl.ds(0, 3)], slot("pairs") + dz)
        top[dz, 2] = paired(dz, tx, upper)
        push("quarters", top.at[dz, 2], in_top.at[dz, 0], summed("tops", dz), e, tx)
        bottom[dz, 2] = paired(dz, ty, lower)
        push("quarters", bottom.at[dz, 2], in_bottom.at[dz, 0], summed("bottoms", dz), e, ty)
        top[dz, 1] = paired(dz, ty, upper)
        bottom[dz, 1] = paired(dz, tx, lower)
        top[dz, 0] = paired(dz, t, upper)
        bottom[dz, 0] = paired(dz, t, lower)

    def second(dz):
        landed(in_top.at[dz, 1], summed("top", dz))
        top[dz, 1] = add(top[dz, 1], in_top[dz, 1]).astype(bf16)
        push("quarters", top.at[dz, 1], last_top.at[dz], summed("last_top", dz), e, ty)
        landed(in_bottom.at[dz, 1], summed("bottom", dz))
        bottom[dz, 1] = add(bottom[dz, 1], in_bottom[dz, 1]).astype(bf16)
        push("quarters", bottom.at[dz, 1], last_bottom.at[dz], summed("last_bottom", dz), e, tx)

    kept = []

    def third(dz):
        for cut, mine, got_in, ending, name in (
                (pl.ds(0, half), top, in_top, last_top, "top"), (pl.ds(half, half), bottom, in_bottom, last_bottom, "bottom")):
            landed(got_in.at[dz, 0], summed(name + "s", dz))
            landed(ending.at[dz], summed("last_" + name, dz))
            value = add(mine[dz, 0], got_in[dz, 0], ending[dz])
            if dz:
                share[dz - 2, cut] = value.astype(bf16)
                push("quarters", share.at[dz - 2, cut], arrived.at[z, cut], slot("share"), back[dz] * 2 + c, t)
            else:
                kept.append(value)

    def wg(i):
        if i < 3:
            right = d_in[...].reshape(ep * rows, 2 * hidden)
            for q in range(i * 2 - 2, i * 2):
                both = tn(full[:, 0, q].reshape(ep * rows, cols), right)
                g_gate[0, pl.ds(q * cols, cols), :] = both[:, :hidden]
                g_up[0, pl.ds(q * cols, cols), :] = both[:, hidden:]
        else:
            left = act_w[...].reshape(ep * rows, hidden)
            for q in range(tp):
                g_down[0, :, pl.ds(q * cols, cols)] = tn(left, full[:, 1, q].reshape(ep * rows, cols))

    def tally():
        score_rows[...] = jnp.concatenate([score[j, :1] for j in range(ep)], axis=0)
        for k in range(1, tp):
            push("small", score_rows, scores.at[t], slot("score"), e, lax.rem(t + k, tp))
        scores[t] = score_rows[...]

    def homeward():
        landed(scores.at[pl.ds(0, tp - 1)], slot("score"))
        total[...] = add(*[scores[j] for j in range(tp)])
        for k in range(1, ep):
            push("home", total, home.at[e], slot("home"), lax.rem(e + k, ep), t)
        home[e] = total[...]

    def finish(count, blocks):
        landed(arrived.at[pl.ds(0, count)], slot("share"))
        for cut, value in zip((upper, lower), kept):
            result[cut] = add(value, *[arrived[back[i], cut] for i in blocks]).astype(bf16)
        kept.clear()

    @pl.when(outer)
    def _():
        for act, *where in (
            (own,), (fwd, 0), (near, 0), (near, 1), (near, 2), (near, 3), (relayx, 1), (near, 4), (relayy, 1),
            (far, 0), (far, 1), (diag, 1), (far, 2), (crossed, 1), (relayx, 2), (far, 3), (last, 0), (fwd, 1),
            (relayy, 2), (last, 1), (bwd, 1), (hand, 1), (crossed, 2), (diag, 2), (last, 2), (far, 4), (relayx, 3),
            (relayy, 3), (fwd, 2), (last, 3), (bwd, 2), (diag, 3), (first, 2), (bwd, 0), (last, 4), (crossed, 3),
            (firstB, 2), (second, 2), (fwd, 3), (bwd, 3), (tally,), (first, 3), (third, 2), (wg, 1), (firstB, 3),
            (second, 3), (first, 0), (firstB, 0), (wg, 2), (homeward,), (wg, 3), (third, 3), (second, 0), (third, 0),
        ):
            with jax.named_scope(act.__name__):
                act(*where)
        finish(nz - 1, (1, 2, 3))

    @pl.when(middle)
    def _():
        onto.update({1: behind, 2: behind, 3: ahead})
        for act, *where in (
            (own,), (last, 0), (near, 0), (near, 1), (near, 2), (last, 1), (relayx, 1), (near, 3), (relayy, 1),
            (far, 0), (last, 2), (relayx, 3), (last, 3), (relayy, 3), (far, 1), (fwd, 0), (crossed, 1), (diag, 1),
            (far, 2), (near, 4), (fwd, 1), (last, 4), (far, 3), (bwd, 0), (relayx, 2), (bwd, 1), (crossed, 3),
            (diag, 3), (hand, 1), (relayy, 2), (far, 4), (fwd, 3), (bwd, 3), (first, 3), (crossed, 2), (diag, 2),
            (firstB, 3), (fwd, 2), (second, 3), (bwd, 2), (tally,), (first, 2), (wg, 3), (firstB, 2), (third, 3),
            (wg, 1), (second, 2), (homeward,), (wg, 2), (first, 0), (firstB, 0), (third, 2), (second, 0), (third, 0),
        ):
            with jax.named_scope(act.__name__):
                act(*where)
        finish(1, (2,))

    landed(home.at[pl.ds(0, ep - 1)], slot("home"))
    back_home = jnp.concatenate(
        [jnp.sum(jnp.where(named == e, home[j], 0.0), axis=0, keepdims=True) for j in range(ep)], axis=0)
    for k, hit in enumerate(hits):
        out_home[pl.ds(k, 1), :] = jnp.sum(jnp.where(hit, back_home, 0.0), axis=0, keepdims=True)
    assert sum(n for _, n in names.values()) == got.shape[0]
    drained("pair", other)
    drained("plane", full.at[pl.ds(0, 3), 0])
    drained("side", full.at[pl.ds(0, 4)])
    drained("own", full.at[0, 0, pl.ds(0, 3)])
    drained("hand", full.at[0, 0])
    drained("quarters", full.at[pl.ds(0, 7), 0, pl.ds(0, 2)])
    drained("home", weights.at[pl.ds(0, ep - 1)])
    drained("small", weights)

    @pl.when(middle)
    def _():
        drained("relay", full.at[pl.ds(0, 3), 0])
        drained("relay_w", weights.at[pl.ds(0, 4)])


def deliver(*refs):
    half = (len(refs) - 1) // 2
    copies = [pltpu.make_async_copy(src, dst, refs[-1].at[i])
              for i, (src, dst) in enumerate(zip(refs[:half], refs[half:-1]))]
    for copy in copies:
        copy.start()
    for copy in copies:
        copy.wait()


def dense(tokens, cotangent, routes, route_weight, w_gate, w_up, w_down):
    f32, bf16 = jnp.float32, jnp.bfloat16
    rows, width = tokens.shape
    ep, tp = lax.axis_size("ep"), lax.axis_size("tp")
    cols, half, nz, hidden = width // tp, rows // 2, ep // 2, w_gate.shape[2]
    anywhere, near = pl.BlockSpec(memory_space=pltpu.HBM), pl.BlockSpec(memory_space=pltpu.VMEM)

    def held(space, *arrays):
        return [pltpu.with_memory_space_constraint(x, space) for x in arrays]

    shapes = ((rows, cols), bf16), (routes.T.shape, f32), (w_gate.shape, f32), (w_up.shape, f32), (w_down.shape, f32)
    parts = pl.pallas_call(
        functools.partial(kernel, ep, tp),
        out_shape=tuple(pltpu.VMEM(*shape) for shape in shapes),
        in_specs=[anywhere, anywhere, near, near, anywhere, anywhere, anywhere],
        out_specs=(near,) * 5,
        scratch_shapes=[
            pltpu.VMEM((ep, 2, tp, rows, cols), bf16),
            pltpu.VMEM((width, 2 * hidden), bf16),
            pltpu.VMEM((hidden, width), bf16),
            pltpu.VMEM((ep, ep, rows), f32),
            pltpu.VMEM((ep, tp, rows, cols), bf16),
            pltpu.VMEM((nz, tp, rows, cols), bf16),
            pltpu.VMEM((nz, 4, half, cols), bf16),
            pltpu.VMEM((nz, 4, half, cols), bf16),
            pltpu.VMEM((nz, 2, half, cols), bf16),
            pltpu.VMEM((nz, 2, half, cols), bf16),
            pltpu.VMEM((nz, half, cols), bf16),
            pltpu.VMEM((nz, half, cols), bf16),
            pltpu.VMEM((2, rows, cols), bf16),
            pltpu.VMEM((nz, rows, cols), bf16),
            pltpu.VMEM((2, tp, rows, cols), bf16),
            pltpu.VMEM((ep, rows, 2 * hidden), bf16),
            pltpu.VMEM((ep, rows, hidden), bf16),
            pltpu.VMEM((ep, 8, rows), f32),
            pltpu.VMEM((ep, rows), f32),
            pltpu.VMEM((tp, ep, rows), f32),
            pltpu.VMEM((ep, rows), f32),
            pltpu.VMEM((ep, ep, rows), f32),
            pltpu.SemaphoreType.DMA((4,)),
            pltpu.SemaphoreType.DMA((10,)),
            pltpu.SemaphoreType.DMA((86,)),
        ],
        compiler_params=pltpu.CompilerParams(
            collective_id=0, has_side_effects=True, vmem_limit_bytes=50 * 1024 * 1024),
    )(*held(pltpu.HBM, tokens, cotangent), routes.T, route_weight.T,
      *held(pltpu.HBM, w_gate, w_up, w_down))
    grad_tokens, grw, *grads = pl.pallas_call(
        deliver,
        out_shape=tuple(jax.ShapeDtypeStruct(*shape) for shape in shapes),
        in_specs=[near] * 5,
        out_specs=(anywhere,) * 5,
        scratch_shapes=[pltpu.SemaphoreType.DMA((5,))],
        compiler_params=pltpu.CompilerParams(vmem_limit_bytes=1 << 20),
    )(*held(pltpu.VMEM, *parts))
    return grad_tokens, grw.T, *grads


def on_device(*args):
    rows, width = args[0].shape
    ep, tp = lax.axis_size("ep"), lax.axis_size("tp")
    fits = tp == 4 and ep == 8 and rows % 128 == 0 and 4 * rows * width * ep <= 1 << 24
    return (dense if fits else slotted)(*args)


def solution(mesh):
    return jax.shard_map(
        on_device,
        mesh=mesh,
        in_specs=(
            P("ep", None),
            P("ep", None),
            P("ep", None),
            P("ep", None),
            P("ep", None, "tp"),
            P("ep", None, "tp"),
            P("ep", "tp", None),
        ),
        out_specs=(
            P("ep", "tp"),
            P("ep", None),
            P("ep", None, "tp"),
            P("ep", None, "tp"),
            P("ep", "tp", None),
        ),
        check_vma=False,
    )
```

time: 60.7 us -> 57.7 us (0.951)
  Pallas kernels: 59.9 us -> 56.7 us
    pallas_call x1, Pallas kernels: 57.1 us -> 53.9 us  [dense(): pl.pallas_call(functools.partial(kernel, ep, tp), out_shape=tuple((pltpu....]
where the time goes in v4:
time: 57.7 us; the launch traced here: 57.5 us
  Pallas kernels  56.7 us (98%)
  between operations  0.8 us (1%)
    pallas_call x1, Pallas kernels, dense(): pl.pallas_call(functools.partial(kernel, ep, tp), out_shape=tuple((pltpu....  53.9 us
    pallas_call x1, Pallas kernels, dense(): pl.pallas_call(deliver, out_shape=tuple((jax.ShapeDtypeStruct(*shape) for...  2.79 us

profile of v4, /device:TPU:0, one launch (start us, length us, event | category | flops | bytes accessed | tf_op | source)
XLA Modules:
  0.0 57.5 jit_solution(10308340783952036105)
XLA Ops:
  0.6 53.9 %shard_map.110 = (bf16[128,512]{1,0:T(8,128)(2,1)S(1)}, f32[2,128]{1,0:T(2,128)S(1)}, f32[1,2048,256]{2,1,0:T(8,128)S(1)}, f32[1,2048,256]{2,1,0:T(8,128)S(1)}, f32[1,256,2048]{2,1,0:T(8,128)S(1)}) custom-call(bf16[128,2048]{1,0:T(8,128)(2,1)} %tokens.1, bf16[128,2048]{1,0:T(8,128)(2,1)} %cotangent.1, s32[2,128]{1,0:T(2,128)} %bitcast.3, f32[2,128]{1,0:T(2,128)} %bitcast.4, ...), custom_call_target="tpu_custom_call" | custom-call | tf_op jit(solution)/shard_map/pallas_call | solution.py:496
  54.5 2.8 %shard_map.111 = (bf16[128,512]{1,0:T(8,128)(2,1)}, f32[2,128]{1,0:T(2,128)}, f32[1,2048,256]{2,1,0:T(8,128)}, f32[1,2048,256]{2,1,0:T(8,128)}, f32[1,256,2048]{2,1,0:T(8,128)}) custom-call(bf16[128,512]{1,0:T(8,128)(2,1)S(1)} %get-tuple-element.15.refs_0_, f32[2,128]{1,0:T(2,128)S(1)} %get-tuple-element.16.refs_1_, ...), custom_call_target="tpu_custom_call" | custom-call | tf_op jit(solution)/shard_map/pallas_call | solution.py:532

commit v5 on v4

--- a/solution.py
+++ b/solution.py
@@ -104,11 +104,11 @@
     return (grad_tokens, grad_route_weight, grad_gate, grad_up, grad_down)
 
 
-def kernel(ep, tp, tokens, cotangent, routes, route_weight, w_gate, w_up, w_down,
+def kernel(ep, tp, tokens, cotangent, routes_in, weight_in, w_gate, w_up, w_down,
            result, out_home, g_gate, g_up, g_down,
            full, in_v, down_v, weights, part, other, top, bottom,
            in_top, in_bottom, last_top, last_bottom, share, arrived, early,
-           d_in, act_w, score, score_rows, scores, total, home,
+           d_in, act_w, score, score_rows, scores, total, home, routes, route_weight,
            local, sent, got):
     f32, bf16 = jnp.float32, jnp.bfloat16
     rows, width = tokens.shape
@@ -162,9 +162,15 @@
         pl.semaphore_signal(barrier, inc=1, device_id={"ep": to_e, "tp": to_t},
                             device_id_type=pl.DeviceIdType.MESH)
 
-    own_tiles = [pltpu.make_async_copy(ref.at[:, pl.ds(q * cols, cols)], full.at[e, a, q], local.at[0])
-                 for a, ref in enumerate((tokens, cotangent)) for q in range(tp)]
-    for copy in own_tiles:
+    for a, turn in ((0, 0), (1, 0), (1, 3), (0, 1), (0, 2), (0, 3), (1, 1), (1, 2)):
+        q = (t, tx, ty, td)[turn]
+        ref = (tokens, cotangent)[a]
+        pltpu.make_async_copy(
+            ref.at[:, pl.ds(pl.multiple_of(q * cols, cols), cols)], full.at[e, a, q],
+            local.at[(a if turn in (0, 3 * a) else 5 + a)]).start()
+    small = [pltpu.make_async_copy(src, dst, local.at[7 + i])
+             for i, (src, dst) in enumerate(((routes_in, routes), (weight_in, route_weight)))]
+    for copy in small:
         copy.start()
     greet(ahead * 2 + c, t)
     pl.when(middle)(lambda: greet(behind * 2 + c, t))
@@ -180,10 +186,6 @@
     def summed(name, dz):
         return slot(name) + max(dz - 1, 0)
 
-    named = lax.broadcasted_iota(jnp.int32, (ep, rows), 0)
-    hits = [named == routes[pl.ds(k, 1), :] for k in range(routes.shape[0])]
-    weights[e] = sum(jnp.where(hit, route_weight[pl.ds(k, 1), :], 0.0) for k, hit in enumerate(hits))
-    pltpu.make_async_copy(full.at[e], full.at[e], local.at[0]).wait()
     pl.semaphore_wait(barrier, jnp.where(middle, 5, 4))
 
     def pieces(s):
@@ -193,13 +195,28 @@
     def along(block, k):
         return slot("along") + block * 6 + k
 
+    def loaded(ref, i):
+        pltpu.make_async_copy(ref, ref, local.at[i]).wait()
+
     for k, piece in enumerate(pieces(e)):
+        if k == 0:
+            loaded(full.at[e, 0, 0], 0)
+        elif k == 2:
+            loaded(full.at[e, 1, pl.ds(0, 2)], 1)
+        elif k == 5:
+            for copy in small:
+                copy.wait()
+            named = lax.broadcasted_iota(jnp.int32, (ep, rows), 0)
+            hits = [named == routes[pl.ds(i, 1), :] for i in range(routes.shape[0])]
+            weights[e] = sum(jnp.where(hit, route_weight[pl.ds(i, 1), :], 0.0) for i, hit in enumerate(hits))
         push("small" if k == 5 else "own", piece, piece, along(z, k), ahead * 2 + c, t)
         copy = plan("relay_w" if k == 5 else "relay", piece, piece, along(z, k), behind * 2 + c, t)
         pl.when(middle)(copy.start)
     hidden = down_v.shape[0]
+    loaded(full.at[e, 0, pl.ds(0, 3)], 5)
+    loaded(full.at[e, 1, pl.ds(0, 2)], 6)
     loads = [pltpu.make_async_copy(src.at[0], dst, local.at[1 + i]) for i, (src, dst) in enumerate((
-        (w_gate, in_v.at[:, pl.ds(0, hidden)]), (w_up, in_v.at[:, pl.ds(hidden, hidden)]), (w_down, down_v)))]
+        (w_gate, in_v.at[:, pl.ds(0, hidden)]), (w_up, in_v.at[:, pl.ds(hidden, hidden)]), (w_down, down_v)), 1)]
     for copy in loads:
         copy.start()
 
@@ -216,13 +233,11 @@
     onto = {}
 
     def step(dz, k):
-        if k == 6:
-            return
         block = back[dz]
         s = block * 2 + c
         piece = pieces(s)[k]
         landed(piece, along(block, k))
-        if dz in onto:
+        if dz in onto and dz > 1:
             push("relay_w" if k == 5 else "relay", piece, piece, along(block, k), onto[dz] * 2 + c, t)
         if k < 4:
             to = dz * 3 - 3 + min(k, 2)
@@ -238,6 +253,11 @@
 
     def near(k):
         step(1, k)
+
+    def pass_on(k):
+        for i in (4, 5) if k == 4 else (k,):
+            piece = pieces(back[1] * 2 + c)[i]
+            push("relay_w" if i == 5 else "relay", piece, piece, along(back[1], i), behind * 2 + c, t)
 
     def far(k):
         step(2, k)
@@ -425,12 +445,12 @@
     @pl.when(outer)
     def _():
         for act, *where in (
-            (own,), (fwd, 0), (near, 0), (near, 1), (near, 2), (near, 3), (relayx, 1), (near, 4), (relayy, 1),
-            (far, 0), (far, 1), (diag, 1), (far, 2), (crossed, 1), (relayx, 2), (far, 3), (last, 0), (fwd, 1),
-            (relayy, 2), (last, 1), (bwd, 1), (hand, 1), (crossed, 2), (diag, 2), (last, 2), (far, 4), (relayx, 3),
-            (relayy, 3), (fwd, 2), (last, 3), (bwd, 2), (diag, 3), (first, 2), (bwd, 0), (last, 4), (crossed, 3),
-            (firstB, 2), (second, 2), (fwd, 3), (bwd, 3), (tally,), (first, 3), (third, 2), (wg, 1), (firstB, 3),
-            (second, 3), (first, 0), (firstB, 0), (wg, 2), (homeward,), (wg, 3), (third, 3), (second, 0), (third, 0),
+            (near, 0), (own,), (near, 1), (relayx, 1), (near, 2), (near, 3), (fwd, 0), (relayy, 1), (far, 0),
+            (far, 1), (far, 2), (diag, 1), (near, 4), (crossed, 1), (last, 0), (far, 3), (fwd, 1), (relayx, 2),
+            (relayy, 2), (last, 1), (bwd, 1), (hand, 1), (crossed, 2), (relayx, 3), (diag, 2), (last, 2), (far, 4),
+            (relayy, 3), (fwd, 2), (last, 3), (bwd, 2), (first, 2), (last, 4), (crossed, 3), (diag, 3), (firstB, 2),
+            (bwd, 0), (second, 2), (fwd, 3), (first, 0), (bwd, 3), (tally,), (first, 3), (third, 2), (firstB, 3),
+            (second, 3), (wg, 2), (firstB, 0), (second, 0), (wg, 3), (third, 3), (homeward,), (wg, 1), (third, 0),
         ):
             with jax.named_scope(act.__name__):
                 act(*where)
@@ -438,14 +458,15 @@
 
     @pl.when(middle)
     def _():
-        onto.update({1: behind, 2: behind, 3: ahead})
+        onto.update({2: behind, 3: ahead})
         for act, *where in (
-            (own,), (last, 0), (near, 0), (near, 1), (near, 2), (last, 1), (relayx, 1), (near, 3), (relayy, 1),
-            (far, 0), (last, 2), (relayx, 3), (last, 3), (relayy, 3), (far, 1), (fwd, 0), (crossed, 1), (diag, 1),
-            (far, 2), (near, 4), (fwd, 1), (last, 4), (far, 3), (bwd, 0), (relayx, 2), (bwd, 1), (crossed, 3),
-            (diag, 3), (hand, 1), (relayy, 2), (far, 4), (fwd, 3), (bwd, 3), (first, 3), (crossed, 2), (diag, 2),
-            (firstB, 3), (fwd, 2), (second, 3), (bwd, 2), (tally,), (first, 2), (wg, 3), (firstB, 2), (third, 3),
-            (wg, 1), (second, 2), (homeward,), (wg, 2), (first, 0), (firstB, 0), (third, 2), (second, 0), (third, 0),
+            (last, 0), (near, 0), (own,), (near, 1), (pass_on, 0), (last, 1), (near, 2), (relayx, 1), (near, 3),
+            (pass_on, 1), (relayy, 1), (relayx, 3), (pass_on, 2), (last, 2), (far, 0), (pass_on, 3), (relayy, 3),
+            (last, 3), (far, 1), (near, 4), (diag, 1), (far, 2), (crossed, 1), (last, 4), (pass_on, 4), (far, 3),
+            (fwd, 1), (bwd, 1), (hand, 1), (crossed, 3), (diag, 3), (far, 4), (fwd, 0), (relayx, 2), (relayy, 2),
+            (fwd, 3), (bwd, 3), (first, 3), (crossed, 2), (diag, 2), (firstB, 3), (fwd, 2), (second, 3), (bwd, 2),
+            (first, 2), (bwd, 0), (tally,), (third, 3), (firstB, 2), (second, 2), (first, 0), (firstB, 0), (wg, 2),
+            (third, 2), (second, 0), (wg, 3), (homeward,), (wg, 1), (third, 0),
         ):
             with jax.named_scope(act.__name__):
                 act(*where)
@@ -496,7 +517,7 @@
     parts = pl.pallas_call(
         functools.partial(kernel, ep, tp),
         out_shape=tuple(pltpu.VMEM(*shape) for shape in shapes),
-        in_specs=[anywhere, anywhere, near, near, anywhere, anywhere, anywhere],
+        in_specs=[anywhere] * 7,
         out_specs=(near,) * 5,
         scratch_shapes=[
             pltpu.VMEM((ep, 2, tp, rows, cols), bf16),
@@ -521,14 +542,15 @@
             pltpu.VMEM((tp, ep, rows), f32),
             pltpu.VMEM((ep, rows), f32),
             pltpu.VMEM((ep, ep, rows), f32),
-            pltpu.SemaphoreType.DMA((4,)),
+            pltpu.VMEM(routes.T.shape, routes.dtype),
+            pltpu.VMEM(routes.T.shape, f32),
+            pltpu.SemaphoreType.DMA((9,)),
             pltpu.SemaphoreType.DMA((10,)),
             pltpu.SemaphoreType.DMA((86,)),
         ],
         compiler_params=pltpu.CompilerParams(
             collective_id=0, has_side_effects=True, vmem_limit_bytes=50 * 1024 * 1024),
-    )(*held(pltpu.HBM, tokens, cotangent), routes.T, route_weight.T,
-      *held(pltpu.HBM, w_gate, w_up, w_down))
+    )(*held(pltpu.HBM, tokens, cotangent, routes.T, route_weight.T, w_gate, w_up, w_down))
     grad_tokens, grw, *grads = pl.pallas_call(
         deliver,
         out_shape=tuple(jax.ShapeDtypeStruct(*shape) for shape in shapes),

time: 57.7 us -> 57.1 us (0.990)
  Pallas kernels: 56.7 us -> 56.1 us
    pallas_call x1, Pallas kernels: 53.9 us -> 53.3 us  [dense(): pl.pallas_call(functools.partial(kernel, ep, tp), out_shape=tuple((pltpu....]
where the time goes in v5:
time: 57.1 us; the launch traced here: 56.9 us
  Pallas kernels  56.1 us (98%)
  between operations  0.8 us (1%)
    pallas_call x1, Pallas kernels, dense(): pl.pallas_call(functools.partial(kernel, ep, tp), out_shape=tuple((pltpu....  53.3 us
    pallas_call x1, Pallas kernels, dense(): pl.pallas_call(deliver, out_shape=tuple((jax.ShapeDtypeStruct(*shape) for...  2.79 us

profile of v5, /device:TPU:0, one launch (start us, length us, event | category | flops | bytes accessed | tf_op | source)
XLA Modules:
  0.0 56.9 jit_solution(5117069349029916245)
XLA Ops:
  0.6 53.3 %shard_map.110 = (bf16[128,512]{1,0:T(8,128)(2,1)S(1)}, f32[2,128]{1,0:T(2,128)S(1)}, f32[1,2048,256]{2,1,0:T(8,128)S(1)}, f32[1,2048,256]{2,1,0:T(8,128)S(1)}, f32[1,256,2048]{2,1,0:T(8,128)S(1)}) custom-call(bf16[128,2048]{1,0:T(8,128)(2,1)} %tokens.1, bf16[128,2048]{1,0:T(8,128)(2,1)} %cotangent.1, s32[2,128]{1,0:T(2,128)} %bitcast.3, f32[2,128]{1,0:T(2,128)} %bitcast.4, ...), custom_call_target="tpu_custom_call" | custom-call | tf_op jit(solution)/shard_map/pallas_call | solution.py:517
  54.0 2.8 %shard_map.111 = (bf16[128,512]{1,0:T(8,128)(2,1)}, f32[2,128]{1,0:T(2,128)}, f32[1,2048,256]{2,1,0:T(8,128)}, f32[1,2048,256]{2,1,0:T(8,128)}, f32[1,256,2048]{2,1,0:T(8,128)}) custom-call(bf16[128,512]{1,0:T(8,128)(2,1)S(1)} %get-tuple-element.15.refs_0_, f32[2,128]{1,0:T(2,128)S(1)} %get-tuple-element.16.refs_1_, ...), custom_call_target="tpu_custom_call" | custom-call | tf_op jit(solution)/shard_map/pallas_call | solution.py:554

commit v6 on v5

--- a/solution.py
+++ b/solution.py
@@ -450,7 +450,7 @@
             (relayy, 2), (last, 1), (bwd, 1), (hand, 1), (crossed, 2), (relayx, 3), (diag, 2), (last, 2), (far, 4),
             (relayy, 3), (fwd, 2), (last, 3), (bwd, 2), (first, 2), (last, 4), (crossed, 3), (diag, 3), (firstB, 2),
             (bwd, 0), (second, 2), (fwd, 3), (first, 0), (bwd, 3), (tally,), (first, 3), (third, 2), (firstB, 3),
-            (second, 3), (wg, 2), (firstB, 0), (second, 0), (wg, 3), (third, 3), (homeward,), (wg, 1), (third, 0),
+            (second, 3), (wg, 2), (firstB, 0), (third, 3), (second, 0), (wg, 3), (homeward,), (wg, 1), (third, 0),
         ):
             with jax.named_scope(act.__name__):
                 act(*where)

time: 57.1 us -> 57.1 us (level)
  no operation moved by 1% of the time
where the time goes in v6:
time: 57.1 us; the launch traced here: 56.9 us
  Pallas kernels  56.1 us (98%)
  between operations  0.8 us (1%)
    pallas_call x1, Pallas kernels, dense(): pl.pallas_call(functools.partial(kernel, ep, tp), out_shape=tuple((pltpu....  53.3 us
    pallas_call x1, Pallas kernels, dense(): pl.pallas_call(deliver, out_shape=tuple((jax.ShapeDtypeStruct(*shape) for...  2.79 us

profile of v6, /device:TPU:0, one launch (start us, length us, event | category | flops | bytes accessed | tf_op | source)
XLA Modules:
  0.0 56.9 jit_solution(18403033803565550415)
XLA Ops:
  0.6 53.3 %shard_map.110 = (bf16[128,512]{1,0:T(8,128)(2,1)S(1)}, f32[2,128]{1,0:T(2,128)S(1)}, f32[1,2048,256]{2,1,0:T(8,128)S(1)}, f32[1,2048,256]{2,1,0:T(8,128)S(1)}, f32[1,256,2048]{2,1,0:T(8,128)S(1)}) custom-call(bf16[128,2048]{1,0:T(8,128)(2,1)} %tokens.1, bf16[128,2048]{1,0:T(8,128)(2,1)} %cotangent.1, s32[2,128]{1,0:T(2,128)} %bitcast.3, f32[2,128]{1,0:T(2,128)} %bitcast.4, ...), custom_call_target="tpu_custom_call" | custom-call | tf_op jit(solution)/shard_map/pallas_call | solution.py:517
  53.9 2.8 %shard_map.111 = (bf16[128,512]{1,0:T(8,128)(2,1)}, f32[2,128]{1,0:T(2,128)}, f32[1,2048,256]{2,1,0:T(8,128)}, f32[1,2048,256]{2,1,0:T(8,128)}, f32[1,256,2048]{2,1,0:T(8,128)}) custom-call(bf16[128,512]{1,0:T(8,128)(2,1)S(1)} %get-tuple-element.15.refs_0_, f32[2,128]{1,0:T(2,128)S(1)} %get-tuple-element.16.refs_1_, ...), custom_call_target="tpu_custom_call" | custom-call | tf_op jit(solution)/shard_map/pallas_call | solution.py:554
